TPU v7x, 512 devices: a whole 4x4x16 slice. The times are simulated.
512 devices in a mesh: ep: 32 (over z, core), tp: 16 (over y, x).
Axes of the slice: x: 4, y: 4, z: 16, core: 2. Of those that a mesh axis runs over, the one named last changes fastest.
Arguments:
- tokens: bfloat16 [4096, 4096], P('ep', 'tp'), may hold values from -6 to 6
- out_grad: bfloat16 [4096, 4096], P('ep', 'tp'), may hold values from -1.5 to 1.5
- routes: int32 [4096, 2], P('ep'), may hold values from 0 to 31, all different within a row; in each aligned block of 128 rows (0 to 127, 128 to 255, ...) at most 10 rows name the same one
- route_weights: float32 [4096, 2], P('ep'), may hold values from 0.2 to 1.2
- gate_proj: bfloat16 [32, 1024, 4096], P('ep', 'tp'), may hold values from -0.09375 to 0.09375
- up_proj: bfloat16 [32, 1024, 4096], P('ep', 'tp'), may hold values from -0.09375 to 0.09375
- down_proj: bfloat16 [32, 1024, 4096], P('ep', 'tp'), may hold values from -0.1875 to 0.1875
- shared_hidden: bfloat16 [4096, 1024], P('ep'), may hold values from -6 to 6
Outputs:
- token_grad: bfloat16 [4096, 4096], P('ep', 'tp')
- weight_grad: float32 [4096, 2], P('ep')
- gate_grad: bfloat16 [32, 1024, 4096], P('ep', 'tp')
- up_grad: bfloat16 [32, 1024, 4096], P('ep', 'tp')
- down_grad: bfloat16 [32, 1024, 4096], P('ep', 'tp')
- shared_grad: float32 [1024, 4096], P('ep', 'tp')
Inputs may be any that keep to these rules, and one draw needn't show every extreme that they name: Within each block of 128 consecutive tokens, no expert is named by more than 10 routes, and in some blocks one expert is named by exactly 10. The 2 experts of one token differ.
All inputs are finite; a program needn't handle non-finite values.
Results may differ from a plain program's by a relative error of at most 0.0065.
Values may be sent and summed in bfloat16 or wider, within the bound.
A program may use at most 64 MiB of HBM per device.

v0:
```python
import jax
import jax.numpy as jnp
from jax import lax
from jax.sharding import Mesh
from jax.sharding import PartitionSpec as P

TP = ("tp_0", "tp_1")


def in_one_piece(arrays, axis, split_dim, concat_dim, along):
    columns = [a.reshape(*a.shape[:along], -1) for a in arrays]
    both = jnp.concatenate(columns, axis=along)
    out, at, finished = (
        lax.all_to_all(both, axis, split_axis=split_dim, concat_axis=concat_dim, tiled=True),
        0,
        [],
    )
    for a, column in zip(arrays, columns):
        share = out[..., at : at + column.shape[along]]
        finished.append(share.reshape(*share.shape[:along], *a.shape[along:]))
        at += column.shape[along]
    return tuple(finished)


def sent_together(arrays, axis, dim, along):
    ends, at = ([], 0)
    for a in arrays[:-1]:
        at += a.shape[along]
        ends.append(at)
    both = jnp.concatenate(arrays, axis=along)
    return tuple(jnp.split(lax.all_gather(both, axis, axis=dim, tiled=True), ends, axis=along))


def cut_along(x, dim, devices):
    before, after = (x.shape[:dim], x.shape[dim + 1 :])
    return jnp.moveaxis(x.reshape(*before, devices, -1, *after), dim, 0)


def cut_rows(length, count):
    lap = length // count
    if lap >= 8:
        lap -= lap % 8
    return [lap * k for k in range(1, count)]


def in_order(blocks, dim):
    dims = list(blocks.shape[1:])
    dims[dim] *= blocks.shape[0]
    return jnp.moveaxis(blocks, 0, dim).reshape(dims)


def several_exchanges(x, axis, pieces, split_dim, concat_dim):
    blocks = cut_along(x, split_dim, lax.axis_size(axis))
    widest = max(range(1, max(2, blocks.ndim - 1)), key=lambda d: blocks.shape[d])
    finished = []
    for share in jnp.split(blocks, cut_rows(blocks.shape[widest], pieces), axis=widest):
        if share.size:
            finished.append(lax.all_to_all(share, axis, split_axis=0, concat_axis=0, tiled=True))
    return in_order(jnp.concatenate(finished, axis=widest), concat_dim)


def over_axes(x, axes):
    for axis in axes:
        x = lax.psum(x, axis)
    return x


def sent_and_summed(x, axis, dim):
    blocks = cut_along(x, dim, lax.axis_size(axis))
    arrived = lax.all_to_all(blocks, axis, split_axis=0, concat_axis=0, tiled=True)
    return arrived.sum(axis=0)


def slot_tables(routes, num_experts, capacity):
    tok_rows, per_token = routes.shape
    route_count = tok_rows * per_token
    flat_routes = routes.reshape(-1)
    expert_ids = lax.broadcasted_iota(jnp.int32, (route_count, num_experts), 1)
    onehot = (flat_routes[:, None] == expert_ids).astype(jnp.int32)
    slot_rank = jnp.sum((jnp.cumsum(onehot, axis=0) - 1) * onehot, axis=1)
    slot_of_route = flat_routes * capacity + slot_rank
    slot_ids = lax.broadcasted_iota(jnp.int32, (num_experts * capacity, route_count), 0)
    route_ids = lax.broadcasted_iota(jnp.int32, (num_experts * capacity, route_count), 1)
    matches = slot_ids == slot_of_route[None, :]
    route_of_slot = jnp.sum(jnp.where(matches, route_ids, 0), axis=1)
    filled = jnp.any(matches, axis=1)
    return (slot_of_route, route_of_slot, filled)


def local(tokens, out_grad, routes, route_weights, gate_proj, up_proj, down_proj, shared_hidden):
    ep_count = lax.axis_size("ep")
    tp_count = lax.axis_size(TP)
    local_experts = gate_proj.shape[0]
    num_experts = local_experts * ep_count
    tok_rows, per_token = routes.shape
    capacity = max(2, 5 * tok_rows * per_token // (4 * num_experts))
    slot_of_route, route_of_slot, filled = slot_tables(routes, num_experts, capacity)
    token_of_slot = route_of_slot // per_token
    zero_value = jnp.zeros((), jnp.bfloat16)
    slot_weight = jnp.where(filled, route_weights.reshape(-1)[route_of_slot], 0.0)
    slot_weight = slot_weight.astype(jnp.bfloat16).reshape(ep_count, local_experts, capacity)
    layout = (ep_count, local_experts, capacity, -1)
    sent_tokens = jnp.where(filled[:, None], tokens[token_of_slot], zero_value).reshape(layout)
    sent_grads = jnp.where(filled[:, None], out_grad[token_of_slot], zero_value).reshape(layout)
    part_tokens, part_grads, weights_in = in_one_piece(
        (sent_tokens, sent_grads, slot_weight), "ep", 0, 2, 3
    )
    rows_in, grads_in = sent_together((part_tokens, part_grads), TP, 3, 0)
    rows_in = rows_in[0]
    grads_in = grads_in[0]
    slot_scale = weights_in[0].astype(jnp.float32)
    pre_gate = jnp.einsum("lrd,lfd->lrf", rows_in, gate_proj, preferred_element_type=jnp.float32)
    pre_up = jnp.einsum("lrd,lfd->lrf", rows_in, up_proj, preferred_element_type=jnp.float32)
    squash = jax.nn.sigmoid(pre_gate)
    activated = pre_gate * squash
    hidden = (activated * pre_up).astype(jnp.bfloat16)
    back_grad = jnp.einsum("lrd,lfd->lrf", grads_in, down_proj, preferred_element_type=jnp.float32)
    partial_products = jnp.sum(hidden.astype(jnp.float32) * back_grad, axis=2)
    hidden_grad = slot_scale[:, :, None] * back_grad
    scaled_hidden = (slot_scale[:, :, None] * hidden.astype(jnp.float32)).astype(jnp.bfloat16)
    gate_delta = (hidden_grad * pre_up * squash * (1.0 + pre_gate * (1.0 - squash))).astype(
        jnp.bfloat16
    )
    up_delta = (hidden_grad * activated).astype(jnp.bfloat16)
    gate_grad = jnp.einsum(
        "lrf,lrd->lfd", gate_delta, rows_in, preferred_element_type=jnp.float32
    ).astype(jnp.bfloat16)
    up_grad = jnp.einsum(
        "lrf,lrd->lfd", up_delta, rows_in, preferred_element_type=jnp.float32
    ).astype(jnp.bfloat16)
    down_grad = jnp.einsum(
        "lrf,lrd->lfd", scaled_hidden, grads_in, preferred_element_type=jnp.float32
    ).astype(jnp.bfloat16)
    partial_rows = jnp.einsum(
        "lrf,lfd->lrd", gate_delta, gate_proj, preferred_element_type=jnp.float32
    )
    partial_rows = partial_rows + jnp.einsum(
        "lrf,lfd->lrd", up_delta, up_proj, preferred_element_type=jnp.float32
    )
    partial_rows = partial_rows.astype(jnp.bfloat16)
    gathered = several_exchanges(partial_rows, TP, 2, 2, 0)
    gathered = gathered.reshape((tp_count,) + partial_rows.shape[:2] + (-1,))
    summed = jnp.sum(gathered, axis=0, dtype=jnp.float32)
    products = over_axes(partial_products, TP)
    slot_rows, slot_products = in_one_piece((summed[None], products[None]), "ep", 2, 0, 3)
    feature_width = slot_rows.shape[-1]
    slot_rows = slot_rows.reshape(num_experts * capacity, feature_width)
    route_rows = slot_rows[slot_of_route].reshape(tok_rows, per_token, feature_width)
    token_grad = jnp.sum(route_rows, axis=1).astype(jnp.bfloat16)
    weight_grad = slot_products.reshape(-1)[slot_of_route].reshape(tok_rows, per_token)
    shared_grad = sent_and_summed(
        lax.dot_general(
            shared_hidden, out_grad, (((0,), (0,)), ((), ())), preferred_element_type=jnp.float32
        ),
        "ep",
        0,
    )
    return (token_grad, weight_grad, gate_grad, up_grad, down_grad, shared_grad)


def solution(mesh):
    finer = Mesh(mesh.devices.reshape(mesh.shape["ep"], 4, 4), ("ep", "tp_0", "tp_1"))
    in_specs = (
        P("ep", TP),
        P("ep", TP),
        P("ep", None),
        P("ep", None),
        P("ep", TP, None),
        P("ep", TP, None),
        P("ep", TP, None),
        P("ep", None),
    )
    out_specs = (
        P("ep", TP),
        P("ep", None),
        P("ep", TP, None),
        P("ep", TP, None),
        P("ep", TP, None),
        P("ep", TP),
    )
    return jax.shard_map(local, mesh=finer, in_specs=in_specs, out_specs=out_specs, check_vma=False)
```

profile of v0, /device:TPU:1, one launch (start us, length us, event | category | flops | bytes accessed | tf_op | source)
XLA Modules:
  0.0 318.5 jit_solution(10415510260060775038)
XLA Ops:
  7.2 0.8 copy.32
  8.4 0.6 reduce-window.6
  9.0 0.2 slice_reduce_fusion.2
  9.3 0.2 fusion.13
  9.5 0.2 select_reduce_fusion
  9.6 0.8 copy.35
  10.4 0.1 reshape.336
  10.7 2.4 gather_fusion.2
  13.1 0.2 convert_element_type.107
  13.4 2.5 gather_fusion.1
  15.9 2.0 gather_fusion
  18.3 55.5 %all_to_all.39 = bf16[32,1,10,513]{3,2,1,0:T(8,128)(2,1)S(1)} all-to-all(bf16[32,1,10,513]{3,2,1,0:T(8,128)(2,1)S(1)} %maximum_bitcast_fusion), channel_id=1, replica_groups=mesh['ep'=32,'tp_0'=4,'tp_1'=4] {'ep'}, dimensions={0} | all-to-all | bytes 656640 | tf_op jit(solution)/shard_map/all_to_all | solution.py:14
  73.8 0.2 all_to_all.28
  74.1 0.8 pad_maximum_fusion.1
  75.0 67.3 %all-gather.2.cloned.1.call-done = bf16[2,1,320,4096]{3,2,1,0:T(8,128)(2,1)} async-done(((bf16[2,1,320,256]{3,2,1,0:T(8,128)(2,1)}), bf16[2,1,320,4096]{3,2,1,0:T(8,128)(2,1)}) %all-gather.2.cloned.1.call-update) | async-done | bytes 5242896 | tf_op jit(solution)/shard_map/all_gather | solution.py:31
  142.2 2.8 fusion.5
  145.0 0.5 copy-done.3
  145.5 0.9 fusion.6
  146.4 0.1 copy-done.10
  146.5 1.4 fusion.14
  148.0 0.9 fusion.7
  148.8 0.9 fusion
  149.7 0.8 copy.44
  150.6 1.0 copy.47
  151.5 1.3 fusion.24
  152.8 22.5 %all_to_all.40 = bf16[16,1,160,256]{3,2,1,0:T(8,128)(2,1)S(1)} all-to-all(bf16[16,1,160,256]{3,2,1,0:T(8,128)(2,1)S(1)} %get-tuple-element.28), channel_id=1, replica_groups=mesh['ep'=32,'tp_0'=4,'tp_1'=4] {'tp_0','tp_1'}, dimensions={0} | all-to-all | bytes 2621440 | tf_op jit(solution)/shard_map/all_to_all | solution.py:58
  175.3 3.7 %all-to-all-start.2 = ((bf16[16,1,160,256]{3,2,1,0:T(8,128)(2,1)}), bf16[16,1,160,256]{3,2,1,0:T(8,128)(2,1)S(1)}, u32[]{:S(2)}, u32[]{:S(2)}) async-start(bf16[16,1,160,256]{3,2,1,0:T(8,128)(2,1)} %get-tuple-element.29), calls=%async_computation.2 | async-start | bytes 2621440 | tf_op jit(solution)/shard_map/all_to_all | solution.py:58
  179.0 1.3 fusion.26
  180.4 15.6 %all-to-all-done.2 = bf16[16,1,160,256]{3,2,1,0:T(8,128)(2,1)S(1)} async-done(((bf16[16,1,160,256]{3,2,1,0:T(8,128)(2,1)}), bf16[16,1,160,256]{3,2,1,0:T(8,128)(2,1)S(1)}, u32[]{:S(2)}, u32[]{:S(2)}) %all-to-all-start.2) | async-done | bytes 1310752 | tf_op jit(solution)/shard_map/all_to_all | solution.py:58
  195.9 17.1 %all-to-all-start.4 = ((f32[32,32,256]{2,1,0:T(8,128)}), f32[32,32,256]{2,1,0:T(8,128)}, u32[]{:S(2)}, u32[]{:S(2)}) async-start(f32[32,32,256]{2,1,0:T(8,128)} %bitcast.70), calls=%async_computation.4 | async-start | bytes 2097152 | tf_op jit(solution)/shard_map/all_to_all | solution.py:70
  213.0 7.0 %psum.14 = f32[1,320]{1,0:T(1,128)S(1)} all-reduce(f32[1,320]{1,0:T(1,128)S(1)} %reduce_sum.65), channel_id=1, replica_groups=mesh['ep'=32,'tp_0'=4,'tp_1'=4] {'tp_0'}, use_global_device_ids=true, to_apply=%region_7.8 | all-reduce | flops 320 | bytes 2560 | tf_op jit(solution)/shard_map/psum | solution.py:64
  220.0 7.6 %psum.15 = f32[1,1,320,1]{2,3,1,0:T(1,128)S(1)} all-reduce(f32[1,1,320,1]{2,3,1,0:T(1,128)S(1)} %bitcast.74), channel_id=1, replica_groups=mesh['ep'=32,'tp_0'=4,'tp_1'=4] {'tp_1'}, use_global_device_ids=true, to_apply=%region_8.9 | all-reduce | flops 320 | bytes 2560 | tf_op jit(solution)/shard_map/psum | solution.py:64
  227.8 0.4 convert_reduce_fusion
  228.2 0.2 broadcast_in_dim.44
  228.4 1.3 pad_maximum_fusion
  229.7 39.1 %all-to-all-done.4 = f32[32,32,256]{2,1,0:T(8,128)} async-done(((f32[32,32,256]{2,1,0:T(8,128)}), f32[32,32,256]{2,1,0:T(8,128)}, u32[]{:S(2)}, u32[]{:S(2)}) %all-to-all-start.4) | async-done | bytes 1048608 | tf_op jit(solution)/shard_map/all_to_all | solution.py:70
  268.8 4.3 %all-to-all-start.3 = ((f32[1,1,320,257]{3,0,1,2:T(1,128)}), f32[1,1,320,257]{3,0,1,2:T(1,128)S(1)}, u32[]{:S(2)}, u32[]{:S(2)}) async-start(f32[1,1,320,257]{3,0,1,2:T(1,128)} %pad_maximum_fusion), calls=%async_computation.3 | async-start | bytes 983040 | tf_op jit(solution)/shard_map/all_to_all | solution.py:14
  273.3 1.9 reduce_sum.68
  275.2 3.2 fusion.1
  278.4 3.2 fusion.2
  281.6 3.2 fusion.3
  284.8 20.4 %all-to-all-done.3 = f32[1,1,320,257]{3,0,1,2:T(1,128)S(1)} async-done(((f32[1,1,320,257]{3,0,1,2:T(1,128)}), f32[1,1,320,257]{3,0,1,2:T(1,128)S(1)}, u32[]{:S(2)}, u32[]{:S(2)}) %all-to-all-start.3) | async-done | bytes 328992 | tf_op jit(solution)/shard_map/all_to_all | solution.py:14
  305.2 0.6 slice_reduce_fusion.1
  305.8 0.8 slice_reduce_fusion
  306.8 1.9 gather_fusion.4
  308.8 1.0 gather_fusion.3
  309.9 0.9 reduce_sum.67
  311.0 0.6 copy.41
  (50 shorter events, 2.0 us)
Async XLA Ops:
  7.2 135.1 %copy-start = (bf16[1,64,4096]{2,1,0:T(8,128)(2,1)S(1)}, bf16[1,64,4096]{2,1,0:T(8,128)(2,1)}, u32[]{:S(2)}) copy-start(bf16[1,64,4096]{2,1,0:T(8,128)(2,1)} %param.12) | copy-start | bytes 1572868
  7.2 8.7 %copy-start.2 = (bf16[128,256]{1,0:T(8,128)(2,1)S(1)}, bf16[128,256]{1,0:T(8,128)(2,1)}, u32[]{:S(2)}) copy-start(bf16[128,256]{1,0:T(8,128)(2,1)} %param.8) | copy-start | bytes 196612
  7.2 135.0 %all-gather.2.cloned.1.call-start = ((), (), s32[]{:S(2)}) async-start(), calls=%async_computation.5 | async-start | bytes 5570560 | tf_op jit(solution)/shard_map/all_gather | solution.py:31
  74.9 70.1 %copy-start.4 = (bf16[1,64,4096]{2,1,0:T(8,128)(2,1)S(1)}, bf16[1,64,4096]{2,1,0:T(8,128)(2,1)}, u32[]{:S(2)}) copy-start(bf16[1,64,4096]{2,1,0:T(8,128)(2,1)} %param.13) | copy-start | bytes 1572868
  142.2 3.3 %copy-start.3 = (bf16[2,1,320,4096]{3,2,1,0:T(8,128)(2,1)S(1)}, bf16[2,1,320,4096]{3,2,1,0:T(8,128)(2,1)}, u32[]{:S(2)}) copy-start(bf16[2,1,320,4096]{3,2,1,0:T(8,128)(2,1)} %all-gather.2.cloned.1.call-done) | copy-start | bytes 15728644
  145.5 1.0 copy-start.10
  148.0 0.9 copy-start.6
  152.8 26.2 %copy-start.1 = (bf16[128,256]{1,0:T(8,128)(2,1)S(1)}, bf16[128,256]{1,0:T(8,128)(2,1)}, u32[]{:S(2)}) copy-start(bf16[128,256]{1,0:T(8,128)(2,1)} %param.9) | copy-start | bytes 196612
  152.8 26.2 %copy-start.5 = (bf16[128,1024]{1,0:T(8,128)(2,1)S(1)}, bf16[128,1024]{1,0:T(8,128)(2,1)}, u32[]{:S(2)}) copy-start(bf16[128,1024]{1,0:T(8,128)(2,1)} %param.15) | copy-start | bytes 786436
  175.3 20.6 %all-to-all-start.2 = ((bf16[16,1,160,256]{3,2,1,0:T(8,128)(2,1)}), bf16[16,1,160,256]{3,2,1,0:T(8,128)(2,1)S(1)}, u32[]{:S(2)}, u32[]{:S(2)}) async-start(bf16[16,1,160,256]{3,2,1,0:T(8,128)(2,1)} %get-tuple-element.29), calls=%async_computation.2 | async-start | bytes 2621440 | tf_op jit(solution)/shard_map/all_to_all | solution.py:58
  195.9 72.8 %all-to-all-start.4 = ((f32[32,32,256]{2,1,0:T(8,128)}), f32[32,32,256]{2,1,0:T(8,128)}, u32[]{:S(2)}, u32[]{:S(2)}) async-start(f32[32,32,256]{2,1,0:T(8,128)} %bitcast.70), calls=%async_computation.4 | async-start | bytes 2097152 | tf_op jit(solution)/shard_map/all_to_all | solution.py:70
  227.8 45.2 %copy-start.9 = (s32[128,2]{0,1:T(2,128)S(1)}, s32[128,2]{0,1:T(2,128)}, u32[]{:S(2)}) copy-start(s32[128,2]{0,1:T(2,128)} %param.10) | copy-start | bytes 3076
  229.7 48.7 %copy-start.7 = (bf16[320,64]{0,1:T(8,128)(2,1)S(1)}, bf16[320,64]{0,1:T(8,128)(2,1)}, u32[]{:S(2)}) copy-start(bf16[320,64]{0,1:T(8,128)(2,1)} %copy-done.6) | copy-start | bytes 122884
  268.8 36.4 %all-to-all-start.3 = ((f32[1,1,320,257]{3,0,1,2:T(1,128)}), f32[1,1,320,257]{3,0,1,2:T(1,128)S(1)}, u32[]{:S(2)}, u32[]{:S(2)}) async-start(f32[1,1,320,257]{3,0,1,2:T(1,128)} %pad_maximum_fusion), calls=%async_computation.3 | async-start | bytes 983040 | tf_op jit(solution)/shard_map/all_to_all | solution.py:14
  275.2 6.4 %copy-start.8 = (bf16[320,64]{0,1:T(8,128)(2,1)S(1)}, bf16[320,64]{0,1:T(8,128)(2,1)}, u32[]{:S(2)}) copy-start(bf16[320,64]{0,1:T(8,128)(2,1)} %get-tuple-element.27) | copy-start | bytes 122884
Sparse Core Ops, SparseCore 0:
  75.0 67.2 all-gather.1
where the time goes:
time: 319 us; the launch traced here: 318 us
  waiting for transfers between devices  142 us (45%)
  blocking collectives  92.6 us (29%)
  starting transfers between devices  25.1 us (8%)
  local copies, waits for them, and re-layouts  19.7 us (6%)
  matrix products  17.7 us (6%)
  between operations  14.4 us (5%)
  other arithmetic  6.67 us (2%)
    all_gather x1, waiting for transfers between devices, sent_together(): lax.all_gather(both, axis, axis=dim, tiled=True)  67.3 us
    all_to_all x1, blocking collectives, in_one_piece(): lax.all_to_all(both, axis, split_axis=split_dim, concat_axis=concat_dim,...  55.5 us
    all_to_all x1, waiting for transfers between devices, sent_and_summed(): lax.all_to_all(blocks, axis, split_axis=0, concat_axis=0, tiled=True)  39.1 us
    all_to_all x1, blocking collectives, several_exchanges(): lax.all_to_all(share, axis, split_axis=0, concat_axis=0, tiled=True)  22.5 us
    all_to_all x1, waiting for transfers between devices, in_one_piece(): lax.all_to_all(both, axis, split_axis=split_dim, concat_axis=concat_dim,...  20.4 us
    all_to_all x1, starting transfers between devices, sent_and_summed(): lax.all_to_all(blocks, axis, split_axis=0, concat_axis=0, tiled=True)  17.1 us
    all_to_all x1, waiting for transfers between devices, several_exchanges(): lax.all_to_all(share, axis, split_axis=0, concat_axis=0, tiled=True)  15.6 us
    psum x2, blocking collectives, over_axes(): x = lax.psum(x, axis)  14.6 us
  transfers between devices with their start and end apart: 4, of which 4 were waited for; matrix products, arithmetic and copies ran while one was open for 5% of the time, Pallas kernels for 0%

commit v1 on v0

v1 whole, which is shorter than its diff:
```python
import functools

import jax
import jax.numpy as jnp
from jax import lax
from jax.experimental import pallas as pl
from jax.experimental.pallas import tpu as pltpu
from jax.sharding import PartitionSpec as P

MESH = pl.DeviceIdType.MESH
BF = jnp.bfloat16
F32 = jnp.float32
SIDE = 4
HIGH = lax.Precision.HIGHEST


def dot(a, b, da, db, precision=None):
    return lax.dot_general(
        a, b, (((da,), (db,)), ((), ())), preferred_element_type=F32, precision=precision
    )


def iota(shape, dim):
    return lax.broadcasted_iota(jnp.int32, shape, dim)


def kernel(
    zs, cap,
    tok, og, routes, routes_t, rw, rw_t, gate, up, down, sh,
    tg_o, wg_o, gg_o, ug_o, dg_o, sg_o,
    wgu, wdn, sb, xa, dl, hd, dlt, hdt, pr, r1, f1, s0, s1, r2, f2, rt, rh, pb, pz, ph, cm,
    sp, sc, shb, shs,
    w_sem, z_send, z_recv, ag_send, ag_recv, rs_send, rs_recv, rz_send, rz_recv,
    pb_send, pb_recv, pz_send, pz_recv, sc_send, sc_recv, sh_send, sh_recv,
):
    ep, tp = lax.axis_index("ep"), lax.axis_index("tp")
    z, c = ep // 2, lax.rem(ep, 2)
    yx = (tp // SIDE, lax.rem(tp, SIDE))
    n_tp = SIDE * SIDE
    slots = 2 * zs
    rows = slots * cap
    half = rows // 2
    pairs = cap // 2
    quarter = zs // 4
    fe = gate.shape[0]
    n_tok = tok.shape[0]

    def ring(d):
        return lax.rem(z + d + zs, zs)

    def ep_of(d, cd):
        return ring(d) * 2 + lax.rem(c + cd, 2)

    def tp_of(h, dp, ds):
        dy, dx = (ds, dp) if h == 0 else (dp, ds)
        return lax.rem(yx[0] + dy + SIDE, SIDE) * SIDE + lax.rem(yx[1] + dx + SIDE, SIDE)

    def remote(src, dst, ssem, rsem, dev):
        return pltpu.make_async_remote_copy(
            src_ref=src, dst_ref=dst, send_sem=ssem, recv_sem=rsem,
            device_id=dev, device_id_type=MESH,
        )

    def arrived(ref, sem):
        remote(ref, ref, sem, sem, (ep, tp)).wait_recv()

    def left(ref, sem):
        remote(ref, ref, sem, sem, (ep, tp)).wait_send()

    loads = [
        pltpu.make_async_copy(gate, wgu.at[pl.ds(0, fe)], w_sem.at[0]),
        pltpu.make_async_copy(up, wgu.at[pl.ds(fe, fe)], w_sem.at[1]),
        pltpu.make_async_copy(down, wdn, w_sem.at[2]),
    ]
    for load in loads:
        load.start()

    barrier = pltpu.get_barrier_semaphore()
    for d in range(zs):
        for cd in range(2):
            if d or cd:
                pl.semaphore_signal(barrier, inc=1, device_id=(ep_of(d, cd), tp), device_id_type=MESH)
    for dy in range(SIDE):
        for dx in range(SIDE):
            if dy or dx:
                pl.semaphore_signal(barrier, inc=1, device_id=(ep, tp_of(0, dx, dy)), device_id_type=MESH)

    def tables(shape, dim):
        r = iota(shape, dim)
        j = lax.shift_right_logical(r * (65536 // cap + 1), 16)
        e = lax.bitwise_and(z + lax.shift_right_logical(j, 1), zs - 1) * 2 + lax.bitwise_and(c + j, 1)
        return e, (r - cap * j).astype(F32)

    def flag(m):
        return jnp.where(m, 1.0, 0.0).astype(BF)

    def weight(x):
        return x.astype(BF).astype(F32)

    before = flag(iota((n_tok, n_tok), 0) < iota((n_tok, n_tok), 1))
    after = flag(iota((n_tok, n_tok), 0) > iota((n_tok, n_tok), 1))
    e, s = tables((rows, n_tok), 0)
    first = routes_t[0:1, :] == e
    hit = first | (routes_t[1:2, :] == e)
    chosen = hit & (dot(flag(hit), before, 1, 0) == s)
    wt = weight(rw_t[...])
    slot_w = jnp.sum(jnp.where(chosen, jnp.where(first, wt[0:1, :], wt[1:2, :]), 0.0), axis=1, keepdims=True)
    pick = flag(chosen)
    sbv = sb.reshape(4, rows, 128)
    for g in range(2):
        sbv[g] = dot(pick, tok[:, g * 128 : (g + 1) * 128], 1, 0).astype(BF)
        sbv[2 + g] = (slot_w * dot(pick, og[:, g * 128 : (g + 1) * 128], 1, 0)).astype(BF)

    pl.semaphore_wait(barrier, slots - 1 + n_tp - 1)

    def order(chunk):
        ds = [quarter - q for q in range(zs // 2)] if chunk == 0 else [quarter - q for q in range(zs // 2, zs)]
        ds = [(d + zs // 2 - 1) % zs - (zs // 2 - 1) for d in ds]
        return sorted(ds, key=abs)

    def slot_in(d, cd):
        return ((quarter - d) % zs) * 2 + cd - (0 if (quarter - d) % zs < zs // 2 else slots // 2)

    def exchange(chunk):
        for d in order(chunk):
            for cd in (1, 0):
                if d or cd:
                    j = (d % zs) * 2 + cd
                    remote(
                        sb.at[:, pl.ds(j * pairs, pairs)],
                        xa.at[chunk, tp, :, pl.ds(slot_in(d, cd) * pairs, pairs)],
                        z_send, z_recv.at[chunk], (ep_of(d, cd), tp),
                    ).start()

    exchange(0)
    exchange(1)
    xa[0, tp, :, pl.ds(slot_in(0, 0) * pairs, pairs)] = sb[:, pl.ds(0, pairs)]

    share = sg_o.shape[0]
    for b in range(sp.shape[0]):
        for cc in range(2):
            lo = (b * 2 + cc) * share
            if lo % 128 == 0:
                wide = dot(sh[:, lo : lo + 128], og[...], 0, 0)
            sp[b, cc] = wide[lo % 128 : lo % 128 + share]
    remote(sp.at[:, 1 - c], sc, sc_send, sc_recv, (ep_of(0, 1), tp)).start()

    def term(d):
        zz = ring(d)
        return sp[zz, c] + sc[zz]

    far = zs // 2

    def shared(step):
        if step == 0:
            arrived(sc, sc_recv)
        for way, hops in ((0, far), (1, far - 1)):
            sign = 1 if way == 0 else -1
            if step > hops:
                continue
            total = term(sign * (hops - step))
            if step:
                arrived(shb.at[way, step - 1], sh_recv.at[way, step - 1])
                total = total + shb[way, step - 1]
            if step < hops:
                shs[way, step] = total
                remote(
                    shs.at[way, step], shb.at[way, step], sh_send.at[way, step], sh_recv.at[way, step],
                    (ep_of(sign, 0), tp),
                ).start()
            elif way == 1:
                sg_o[...] = total
            else:
                sg_o[...] = sg_o[...] + total - term(0)

    back = (0, -1, 1, 2)

    def gather_send(ch, h, k, kind, t, g0, gn, dev_t):
        ref = xa.at[ch, t, pl.ds(2 * h + g0, gn)]
        remote(ref, ref, ag_send, ag_recv.at[ch, h, k, kind], (ep, dev_t)).start()

    def gather_wait(ch, h, k, kind, g0, gn):
        arrived(xa.at[ch, 0, pl.ds(2 * h + g0, gn)], ag_recv.at[ch, h, k, kind])

    def spread(ch, h, k):
        t = tp_of(h, back[k], 0)
        gather_send(ch, h, k, 0, t, 0, 2, tp_of(h, 0, 1))
        gather_send(ch, h, k, 1, t, 0, 2, tp_of(h, 0, -1))

    def relay(ch, h, k):
        gather_wait(ch, h, k, 0, 0, 2)
        gather_send(ch, h, k, 2, tp_of(h, back[k], -1), 0, 1, tp_of(h, 0, 1))
        gather_wait(ch, h, k, 1, 0, 2)
        gather_send(ch, h, k, 3, tp_of(h, back[k], 1), 1, 1, tp_of(h, 0, -1))

    def g_0(ch):
        arrived(xa.at[ch, 0, :, pl.ds(0, (slots // 2 - (1 if ch == 0 else 0)) * pairs)], z_recv.at[ch])
        for h in range(2):
            gather_send(ch, h, 4, 0, tp, 0, 2, tp_of(h, 1, 0))
            gather_send(ch, h, 4, 1, tp, 0, 2, tp_of(h, -1, 0))
        for h in range(2):
            spread(ch, h, 0)

    def g_1(ch):
        for h in range(2):
            gather_wait(ch, h, 4, 0, 0, 2)
            gather_send(ch, h, 4, 2, tp_of(h, -1, 0), 0, 1, tp_of(h, 1, 0))
            gather_wait(ch, h, 4, 1, 0, 2)
            gather_send(ch, h, 4, 3, tp_of(h, 1, 0), 1, 1, tp_of(h, -1, 0))
        for h in range(2):
            spread(ch, h, 1)
            spread(ch, h, 2)

    def g_2(ch):
        for h in range(2):
            relay(ch, h, 0)
        for h in range(2):
            gather_wait(ch, h, 4, 2, 0, 1)
            gather_wait(ch, h, 4, 3, 1, 1)
            spread(ch, h, 3)

    def g_3(ch):
        for h in range(2):
            relay(ch, h, 1)
            relay(ch, h, 2)

    def g_4(ch):
        for h in range(2):
            relay(ch, h, 3)

    def g_5(ch):
        for h in range(2):
            for k in range(4):
                gather_wait(ch, h, k, 2, 0, 1)
                gather_wait(ch, h, k, 3, 1, 1)

    xav = xa.reshape(2, n_tp, 4, half, 128)
    width = 256

    def expert(ch):
        def sums(i, total):
            a, b = total
            for u in range(4):
                t = i * 4 + u
                cols = pl.ds(pl.multiple_of(t * width, width), width)
                x = jnp.concatenate([xav[ch, t, 0], xav[ch, t, 1]], axis=1)
                y = jnp.concatenate([xav[ch, t, 2], xav[ch, t, 3]], axis=1)
                a = a + dot(x, wgu[:, cols], 1, 1)
                b = b + dot(y, wdn[:, cols], 1, 1)
            return a, b

        start = (jnp.zeros((half, 2 * fe), F32), jnp.zeros((half, fe), F32))
        gu, back_grad = lax.fori_loop(0, n_tp // 4, sums, start)
        pre_gate, pre_up = gu[:, :fe], gu[:, fe:]
        squash = 1.0 / (1.0 + jnp.exp(-pre_gate))
        activated = pre_gate * squash
        hidden = (activated * pre_up).astype(BF)
        gate_delta = back_grad * pre_up * squash * (1.0 + pre_gate * (1.0 - squash))
        at = pl.ds(ch * half, half)
        deltas = jnp.concatenate([gate_delta, back_grad * activated], axis=1)
        dl[at, :] = deltas.astype(BF)
        hd[at, :] = hidden
        product = hidden.astype(F32) * back_grad
        line = dot(jnp.ones((8, fe), F32), product, 1, 1, HIGH)
        pb[tp, pl.ds(ch, 1), pl.ds(0, half)] = line[0:1]

    def parts(ch):
        at = pl.ds(ch * half, half)
        for dy in range(SIDE):
            for dx in range(SIDE):
                t = tp_of(0, dx, dy)
                cols = pl.ds(pl.multiple_of(t * width, width), width)
                out = dot(dl[at, :], wgu[:, cols], 1, 0).astype(BF)
                pr[ch, 0, dx, dy] = out[:, :128]
                pr[ch, 1, dy, dx] = out[:, 128:]

    def add(*xs):
        total = xs[0].astype(F32)
        for x in xs[1:]:
            total = total + x.astype(F32)
        return total

    def sum_send(ch, h, src, buf, i, base, dev_t):
        remote(src, buf.at[ch, h, i], rs_send.at[base // 6], rs_recv.at[ch, h, base + i], (ep, dev_t)).start()

    def sum_wait(ch, h, buf, i, base):
        arrived(buf.at[ch, h, i], rs_recv.at[ch, h, base + i])

    lo, hi = pl.ds(0, 2), pl.ds(2, 2)
    top, low = pl.ds(0, half // 2), pl.ds(half // 2, half // 2)

    def q_0(ch):
        for h in range(2):
            sum_send(ch, h, pr.at[ch, h, 2, lo], r1, 0, 0, tp_of(h, 1, 0))
            sum_send(ch, h, pr.at[ch, h, 2, hi], r1, 1, 0, tp_of(h, -1, 0))
        for h in range(2):
            sum_send(ch, h, pr.at[ch, h, 1, hi], r1, 2, 0, tp_of(h, 1, 0))
            sum_send(ch, h, pr.at[ch, h, 3, lo], r1, 3, 0, tp_of(h, -1, 0))

    def q_1(ch):
        for h in range(2):
            sum_wait(ch, h, r1, 0, 0)
            f1[ch, h, 0] = add(pr[ch, h, 1, lo], r1[ch, h, 0]).astype(BF)
            sum_send(ch, h, f1.at[ch, h, 0], r1, 4, 0, tp_of(h, 1, 0))
            sum_wait(ch, h, r1, 1, 0)
            f1[ch, h, 1] = add(pr[ch, h, 3, hi], r1[ch, h, 1]).astype(BF)
            sum_send(ch, h, f1.at[ch, h, 1], r1, 5, 0, tp_of(h, -1, 0))

    def q_2(ch):
        for h in range(2):
            for i in (3, 2, 4, 5):
                sum_wait(ch, h, r1, i, 0)
            for ds in (2, 1, 3, 0):
                pair = (4, 3) if ds < 2 else (2, 5)
                total = add(pr[ch, h, 0, ds], r1[ch, h, pair[0], ds % 2], r1[ch, h, pair[1], ds % 2])
                if ds:
                    s1[ch, h, ds - 1] = total.astype(BF)
                else:
                    s0[ch, h] = total
            sum_send(ch, h, s1.at[ch, h, 1, top], r2, 0, 6, tp_of(h, 0, 1))
            sum_send(ch, h, s1.at[ch, h, 1, low], r2, 1, 6, tp_of(h, 0, -1))
            sum_send(ch, h, s1.at[ch, h, 0, low], r2, 2, 6, tp_of(h, 0, 1))
            sum_send(ch, h, s1.at[ch, h, 2, top], r2, 3, 6, tp_of(h, 0, -1))

    def q_3(ch):
        for h in range(2):
            sum_wait(ch, h, r2, 0, 6)
            f2[ch, h, 0] = add(s1[ch, h, 0, top], r2[ch, h, 0]).astype(BF)
            sum_send(ch, h, f2.at[ch, h, 0], r2, 4, 6, tp_of(h, 0, 1))
            sum_wait(ch, h, r2, 1, 6)
            f2[ch, h, 1] = add(s1[ch, h, 2, low], r2[ch, h, 1]).astype(BF)
            sum_send(ch, h, f2.at[ch, h, 1], r2, 5, 6, tp_of(h, 0, -1))

    rtv = rt.reshape(2, 2, half, 128)

    def q_4(ch):
        for h in range(2):
            for i in (3, 2, 4, 5):
                sum_wait(ch, h, r2, i, 6)
            rtv[ch, h, top] = add(s0[ch, h, top], r2[ch, h, 4], r2[ch, h, 3]).astype(BF)
            rtv[ch, h, low] = add(s0[ch, h, low], r2[ch, h, 2], r2[ch, h, 5]).astype(BF)
        for d in order(ch)[::-1]:
            for cd in (1, 0):
                here = pl.ds(slot_in(d, cd) * pairs, pairs)
                there = pl.ds(((d % zs) * 2 + cd) * pairs, pairs)
                if d or cd:
                    remote(
                        rt.at[ch, :, here], rh.at[:, there], rz_send, rz_recv, (ep_of(-d, cd), tp)
                    ).start()
                else:
                    rh[:, there] = rt[ch, :, here]

    def product_send():
        for dy in range(SIDE):
            for dx in range(SIDE):
                if dy or dx:
                    remote(pb.at[tp], pb.at[tp], pb_send, pb_recv, (ep, tp_of(0, dx, dy))).start()

    def product_return():
        arrived(pb.at[pl.ds(0, n_tp - 1)], pb_recv)
        for ch in range(2):
            total = pb[0, pl.ds(ch, 1), pl.ds(0, half)]
            for t in range(1, n_tp):
                total = total + pb[t, pl.ds(ch, 1), pl.ds(0, half)]
            r = iota((slots // 2, half), 1)
            j = lax.shift_right_logical(r * (65536 // cap + 1), 16)
            own = jnp.where(j == iota((slots // 2, half), 0), total, 0.0)
            r = iota((half, 128), 0)
            j = lax.shift_right_logical(r * (65536 // cap + 1), 16)
            lane = jnp.where(r - cap * j == iota((half, 128), 1), 1.0, 0.0)
            table = dot(own, lane, 1, 0, HIGH)
            for i in range(slots // 2):
                pz[ch * (slots // 2) + i] = table[i : i + 1]
        for ch in range(2):
            for d in order(ch)[::-1]:
                for cd in (1, 0):
                    i, j = ch * (slots // 2) + slot_in(d, cd), (d % zs) * 2 + cd
                    if d or cd:
                        remote(pz.at[i], ph.at[j], pz_send, pz_recv, (ep_of(-d, cd), tp)).start()
                    else:
                        ph[j] = pz[i]

    def weight_grads(t0, t1):
        def one(t, carry):
            cols = pl.ds(pl.multiple_of(t * width, width), width)
            both = jnp.zeros((2 * fe, width), F32)
            last = jnp.zeros((fe, width), F32)
            for ch in range(2):
                x = jnp.concatenate([xav[ch, t, 0], xav[ch, t, 1]], axis=1)
                y = jnp.concatenate([xav[ch, t, 2], xav[ch, t, 3]], axis=1)
                both = both + dot(dlt[ch], x, 1, 0)
                last = last + dot(hdt[ch], y, 1, 0)
            gg_o[:, cols] = both[:fe].astype(BF)
            ug_o[:, cols] = both[fe:].astype(BF)
            dg_o[:, cols] = last.astype(BF)
            return carry

        lax.fori_loop(t0, t1, one, 0)

    def turned(ch):
        at = pl.ds(ch * half, half)
        dlt[ch] = dl[at, :].astype(F32).T.astype(BF)
        hdt[ch] = hd[at, :].astype(F32).T.astype(BF)

    g_0(0)
    shared(0)
    g_1(0)
    shared(1)
    g_2(0)
    shared(2)
    g_0(1)
    shared(3)
    g_3(0)
    g_1(1)
    shared(4)
    g_4(0)
    g_5(0)
    for load in loads:
        load.wait()
    expert(0)
    shared(5)
    g_2(1)
    parts(0)
    g_3(1)
    shared(6)
    turned(0)
    g_4(1)
    q_0(0)
    shared(7)
    g_5(1)
    expert(1)
    product_send()
    q_1(0)
    parts(1)
    q_0(1)
    shared(8)
    turned(1)
    q_2(0)
    weight_grads(0, 4)
    q_1(1)
    q_3(0)
    weight_grads(4, 7)
    q_4(0)
    q_2(1)
    product_return()
    weight_grads(7, 11)
    q_3(1)
    weight_grads(11, 13)
    q_4(1)
    weight_grads(13, 16)

    e, s = tables((n_tok, rows), 1)
    r0, r1c = routes[:, 0:1], routes[:, 1:2]
    hit = (r0 == e) | (r1c == e)
    cm[...] = flag(hit & (dot(after, flag(hit), 1, 0) == s))
    j = iota((n_tok, slots), 1)
    ej = lax.bitwise_and(z + lax.shift_right_logical(j, 1), zs - 1) * 2 + lax.bitwise_and(c + j, 1)
    seen = dot(after, flag((r0 == ej) | (r1c == ej)), 1, 0)
    wc = weight(rw[...])
    arrived(ph.at[pl.ds(0, slots - 1)], pz_recv)
    table = jnp.concatenate([ph[i] for i in range(slots)], axis=0)
    for k in range(2):
        mine = routes[:, k : k + 1] == ej
        rank = jnp.sum(jnp.where(mine, seen, 0.0), axis=1, keepdims=True)
        found = dot(jnp.where(mine, 1.0, 0.0), table, 1, 0, HIGH)
        lane = iota((n_tok, 128), 1).astype(F32)
        value = jnp.sum(jnp.where(lane == rank, found, 0.0), axis=1, keepdims=True)
        wg_o[:, k : k + 1] = value / wc[:, k : k + 1]
    arrived(rh.at[:, pl.ds(0, (slots - 1) * pairs)], rz_recv)
    rhv = rh.reshape(2, rows, 128)
    for h in range(2):
        tg_o[:, h * 128 : (h + 1) * 128] = dot(cm[...], rhv[h], 1, 0).astype(BF)

    left(sb.at[:, pl.ds(0, (slots - 1) * pairs)], z_send)
    left(xa.at[:, pl.ds(0, n_tp - 1)], ag_send)
    left(r1, rs_send.at[0])
    left(r2, rs_send.at[1])
    left(rh.at[:, pl.ds(0, (slots - 1) * pairs)], rz_send)
    left(pb.at[pl.ds(0, n_tp - 1)], pb_send)
    left(ph.at[pl.ds(0, slots - 1)], pz_send)
    left(sc, sc_send)
    for way, hops in ((0, far), (1, far - 1)):
        for step in range(hops):
            left(shs.at[way, step], sh_send.at[way, step])


def local(zs, tokens, out_grad, routes, route_weights, gate_proj, up_proj, down_proj, shared_hidden):
    n_tok, feat = tokens.shape
    _, fe, width = gate_proj.shape
    slots = 2 * zs
    cap = max(2, 5 * n_tok * routes.shape[1] // (4 * slots))
    rows = slots * cap
    half = rows // 2
    n_tp = SIDE * SIDE
    share = shared_hidden.shape[1] // slots
    far = zs // 2
    vmem = pl.BlockSpec(memory_space=pltpu.VMEM)
    hbm = pl.BlockSpec(memory_space=pl.ANY)
    dma = pltpu.SemaphoreType.DMA
    V = pltpu.VMEM
    out = pl.pallas_call(
        functools.partial(kernel, zs, cap),
        out_shape=(
            jax.ShapeDtypeStruct((n_tok, feat), BF),
            jax.ShapeDtypeStruct((n_tok, 2), F32),
            jax.ShapeDtypeStruct((fe, width), BF),
            jax.ShapeDtypeStruct((fe, width), BF),
            jax.ShapeDtypeStruct((fe, width), BF),
            jax.ShapeDtypeStruct((share, feat), F32),
        ),
        in_specs=[vmem] * 6 + [hbm] * 3 + [vmem],
        out_specs=(vmem,) * 6,
        scratch_shapes=[
            V((2 * fe, width), BF),
            V((fe, width), BF),
            V((4, rows // 2, 2, 128), BF),
            V((2, n_tp, 4, half // 2, 2, 128), BF),
            V((rows, 2 * fe), BF),
            V((rows, fe), BF),
            V((2, 2 * fe, half), BF),
            V((2, fe, half), BF),
            V((2, 2, SIDE, SIDE, half, 128), BF),
            V((2, 2, 6, 2, half, 128), BF),
            V((2, 2, 2, 2, half, 128), BF),
            V((2, 2, half, 128), F32),
            V((2, 2, 3, half, 128), BF),
            V((2, 2, 6, half // 2, 128), BF),
            V((2, 2, 2, half // 2, 128), BF),
            V((2, 2, half // 2, 2, 128), BF),
            V((2, rows // 2, 2, 128), BF),
            V((n_tp, 2, 256), F32),
            V((slots, 1, 128), F32),
            V((slots, 1, 128), F32),
            V((n_tok, rows), BF),
            V((zs, 2, share, feat), F32),
            V((zs, share, feat), F32),
            V((2, far, share, feat), F32),
            V((2, far, share, feat), F32),
            dma((3,)),
            dma, dma((2,)),
            dma, dma((2, 2, 5, 4)),
            dma((2,)), dma((2, 2, 12)),
            dma, dma,
            dma, dma,
            dma, dma,
            dma, dma,
            dma((2, far)), dma((2, far)),
        ],
        compiler_params=pltpu.CompilerParams(collective_id=0, has_side_effects=True),
    )(
        tokens, out_grad, routes, routes.T, route_weights, route_weights.T,
        gate_proj[0], up_proj[0], down_proj[0], shared_hidden,
    )
    tg, wg, gg, ug, dg, sg = out
    return tg, wg, gg[None], ug[None], dg[None], sg


def solution(mesh):
    zs = mesh.shape["ep"] // 2
    features, whole, weights = P("ep", "tp"), P("ep", None), P("ep", "tp", None)
    return jax.shard_map(
        functools.partial(local, zs),
        mesh=mesh,
        in_specs=(features, features, whole, whole, weights, weights, weights, whole),
        out_specs=(features, whole, weights, weights, weights, features),
        check_vma=False,
    )
```

time: 319 us -> 105 us (0.33)
  waiting for transfers between devices: 142 us -> 0 us
  Pallas kernels: 0 us -> 95.3 us
  blocking collectives: 92.6 us -> 0 us
  starting transfers between devices: 25.1 us -> 0 us
  matrix products: 17.7 us -> 0 us
  between operations: 14.4 us -> 0.66 us
  local copies, waits for them, and re-layouts: 19.7 us -> 8.87 us
  other arithmetic: 6.67 us -> 0 us
    pallas_call x0 -> x1, Pallas kernels: none -> 95.3 us  [local(): pl.pallas_call(functools.partial(kernel, zs, cap), out_shape=(jax.ShapeDt...]
    all_to_all x2 -> x0, blocking collectives: 78 us -> none  [the longest x1 55.5 us: in_one_piece(): lax.all_to_all(both, axis, split_axis=split_dim, concat_axis=concat_dim,...]
    all_to_all x3 -> x0, waiting for transfers between devices: 75 us -> none  [the longest x1 39.1 us: sent_and_summed(): lax.all_to_all(blocks, axis, split_axis=0, concat_axis=0, tiled=True)]
    all_gather x1 -> x0, waiting for transfers between devices: 67.3 us -> none  [sent_together(): lax.all_gather(both, axis, axis=dim, tiled=True)]
    all_to_all x3 -> x0, starting transfers between devices: 25.1 us -> none  [the longest x1 17.1 us: sent_and_summed(): lax.all_to_all(blocks, axis, split_axis=0, concat_axis=0, tiled=True)]
    dot_general x9 -> x0, matrix products: 17.7 us -> none  [the longest x1 3.18 us: local(): jnp.einsum('lrf,lrd->lfd', gate_delta, rows_in, preferred_element_type=jn...]
    psum x2 -> x0, blocking collectives: 14.6 us -> none  [over_axes(): x = lax.psum(x, axis)]
    gather x7 -> x0, local copies, waits for them, and re-layouts: 9.9 us -> none  [the longest x2 2.54 us: local(): out_grad[token_of_slot]]
  transfers between devices with their start and end apart: 4 -> 0, of which waited for: 4 -> 0; matrix products, arithmetic and copies ran while one was open for 5% -> 0% of each run, Pallas kernels for 0% -> 0%
where the time goes in v1:
time: 105 us
  Pallas kernels  95.3 us (91%)
  local copies, waits for them, and re-layouts  8.87 us (8%)
    pallas_call x1, Pallas kernels, local(): pl.pallas_call(functools.partial(kernel, zs, cap), out_shape=(jax.ShapeDt...  95.3 us
    unnamed x20, local copies, waits for them, and re-layouts  8.87 us

profile of v1, /device:TPU:1, one launch (start us, length us, event | category | flops | bytes accessed | tf_op | source)
XLA Modules:
  0.0 104.8 jit_solution(9153252972123590255)
XLA Ops:
  0.6 0.0 copy-start.4
  0.6 0.7 copy-done.4
  1.3 0.0 copy-start.5
  1.3 0.7 copy.14.routes
  2.1 0.0 copy-done.5
  2.1 0.7 copy.15.rw
  2.8 95.3 %shard_map.127 = (bf16[128,256]{1,0:T(8,128)(2,1)}, f32[128,2]{1,0:T(8,128)}, bf16[64,4096]{1,0:T(8,128)(2,1)}, bf16[64,4096]{1,0:T(8,128)(2,1)}, bf16[64,4096]{1,0:T(8,128)(2,1)}, /*index=5*/f32[32,256]{1,0:T(8,128)}) custom-call(bf16[128,256]{1,0:T(8,128)(2,1)} %tok.1, bf16[128,256]{1,0:T(8,128)(2,1)} %og.1, s32[128,2]{1,0:T(8,128)} %copy.14.routes, ...), custom_call_target="tpu_custom_call" | custom-call | tf_op jit(solution)/shard_map/pallas_call | solution.py:501
  98.1 0.0 copy-start.2
  98.1 1.5 %copy.16 = f32[128,2]{0,1:T(2,128)} copy(f32[128,2]{1,0:T(8,128)} %get-tuple-element.19) | data formatting | bytes 2048
  99.6 0.0 copy-done.2
  99.6 0.6 copy.22
  100.2 0.0 copy-start.1
  100.2 1.9 %copy.23 = bf16[1,64,4096]{2,1,0:T(8,128)(2,1)} copy(bf16[1,64,4096]{2,1,0:T(8,128)(2,1)} %bitcast.13) | data formatting | bytes 1048576
  102.2 0.0 copy-done.1
  102.2 0.0 copy-start
  102.2 0.8 copy.24
  103.0 0.4 copy-done
  103.4 0.0 copy-start.3
  103.4 0.8 copy.25
  104.2 0.0 copy-done.3
  104.2 0.6 copy.26
Async XLA Ops:
  0.6 0.7 copy-start.4
  1.3 0.7 copy-start.5
  98.1 1.5 %copy-start.2 = (bf16[128,256]{1,0:T(8,128)(2,1)S(1)}, bf16[128,256]{1,0:T(8,128)(2,1)}, u32[]{:S(2)}) copy-start(bf16[128,256]{1,0:T(8,128)(2,1)} %get-tuple-element.30) | copy-start | bytes 196612
  100.2 1.9 %copy-start.1 = (bf16[64,4096]{1,0:T(8,128)(2,1)S(1)}, bf16[64,4096]{1,0:T(8,128)(2,1)}, u32[]{:S(2)}) copy-start(bf16[64,4096]{1,0:T(8,128)(2,1)} %get-tuple-element.15) | copy-start | bytes 1572868
  102.2 1.2 %copy-start = (bf16[64,4096]{1,0:T(8,128)(2,1)S(1)}, bf16[64,4096]{1,0:T(8,128)(2,1)}, u32[]{:S(2)}) copy-start(bf16[64,4096]{1,0:T(8,128)(2,1)} %get-tuple-element.16) | copy-start | bytes 1572868
  103.4 0.8 copy-start.3

commit v2 on v1

--- a/solution.py
+++ b/solution.py
@@ -11,7 +11,15 @@
 BF = jnp.bfloat16
 F32 = jnp.float32
 SIDE = 4
+ORDER = (0, 1, 2, 3)
 HIGH = lax.Precision.HIGHEST
+
+
+def chunks_of(zs):
+    near = sorted(range(1 - zs // 2, zs // 2 + 1), key=lambda d: (abs(d), -d))
+    size = zs // len(ORDER)
+    parts = [near[k * size : (k + 1) * size] for k in range(len(ORDER))]
+    return [parts[k] for k in ORDER]
 
 
 def dot(a, b, da, db, precision=None):
@@ -26,9 +34,9 @@
 
 def kernel(
     zs, cap,
-    tok, og, routes, routes_t, rw, rw_t, gate, up, down, sh,
+    tok_h, og_h, routes_h, rw_h, gate, up, down, sh_h,
     tg_o, wg_o, gg_o, ug_o, dg_o, sg_o,
-    wgu, wdn, sb, xa, dl, hd, dlt, hdt, pr, r1, f1, s0, s1, r2, f2, rt, rh, pb, pz, ph, cm,
+    tok, og, routes_t, rw_t, sh, wgu, wdn, sb, xa, dl, hd, dlt, hdt, pr, r1, f1, s0, s1, r2t, r2l, f2t, f2l, rt, rh, pb, pz, ph, cm,
     sp, sc, shb, shs,
     w_sem, z_send, z_recv, ag_send, ag_recv, rs_send, rs_recv, rz_send, rz_recv,
     pb_send, pb_recv, pz_send, pz_recv, sc_send, sc_recv, sh_send, sh_recv,
@@ -39,9 +47,12 @@
     n_tp = SIDE * SIDE
     slots = 2 * zs
     rows = slots * cap
-    half = rows // 2
+    groups = chunks_of(zs)
+    nch = len(groups)
+    ns = slots // nch
+    half = rows // nch
+    cut = (half // 2 + 15) // 16 * 16
     pairs = cap // 2
-    quarter = zs // 4
     fe = gate.shape[0]
     n_tok = tok.shape[0]
 
@@ -72,7 +83,13 @@
         pltpu.make_async_copy(up, wgu.at[pl.ds(fe, fe)], w_sem.at[1]),
         pltpu.make_async_copy(down, wdn, w_sem.at[2]),
     ]
-    for load in loads:
+    small = [
+        pltpu.make_async_copy(src, dst, w_sem.at[3 + i])
+        for i, (src, dst) in enumerate(
+            ((routes_h, routes_t), (rw_h, rw_t), (tok_h, tok), (og_h, og), (sh_h, sh))
+        )
+    ]
+    for load in small + loads:
         load.start()
 
     barrier = pltpu.get_barrier_semaphore()
@@ -84,6 +101,9 @@
         for dx in range(SIDE):
             if dy or dx:
                 pl.semaphore_signal(barrier, inc=1, device_id=(ep, tp_of(0, dx, dy)), device_id_type=MESH)
+
+    for load in small:
+        load.wait()
 
     def tables(shape, dim):
         r = iota(shape, dim)
@@ -111,18 +131,21 @@
         sbv[g] = dot(pick, tok[:, g * 128 : (g + 1) * 128], 1, 0).astype(BF)
         sbv[2 + g] = (slot_w * dot(pick, og[:, g * 128 : (g + 1) * 128], 1, 0)).astype(BF)
 
+    share = sg_o.shape[0]
+    for b in range(sp.shape[0]):
+        for cc in range(2):
+            lo = (b * 2 + cc) * share
+            if lo % 128 == 0:
+                wide = dot(sh[:, lo : lo + 128], og[...], 0, 0)
+            sp[b, cc] = wide[lo % 128 : lo % 128 + share]
+
     pl.semaphore_wait(barrier, slots - 1 + n_tp - 1)
 
-    def order(chunk):
-        ds = [quarter - q for q in range(zs // 2)] if chunk == 0 else [quarter - q for q in range(zs // 2, zs)]
-        ds = [(d + zs // 2 - 1) % zs - (zs // 2 - 1) for d in ds]
-        return sorted(ds, key=abs)
-
     def slot_in(d, cd):
-        return ((quarter - d) % zs) * 2 + cd - (0 if (quarter - d) % zs < zs // 2 else slots // 2)
+        return [g.index(d) for g in groups if d in g][0] * 2 + cd
 
     def exchange(chunk):
-        for d in order(chunk):
+        for d in groups[chunk]:
             for cd in (1, 0):
                 if d or cd:
                     j = (d % zs) * 2 + cd
@@ -132,17 +155,10 @@
                         z_send, z_recv.at[chunk], (ep_of(d, cd), tp),
                     ).start()
 
-    exchange(0)
-    exchange(1)
+    for ch in range(nch):
+        exchange(ch)
     xa[0, tp, :, pl.ds(slot_in(0, 0) * pairs, pairs)] = sb[:, pl.ds(0, pairs)]
 
-    share = sg_o.shape[0]
-    for b in range(sp.shape[0]):
-        for cc in range(2):
-            lo = (b * 2 + cc) * share
-            if lo % 128 == 0:
-                wide = dot(sh[:, lo : lo + 128], og[...], 0, 0)
-            sp[b, cc] = wide[lo % 128 : lo % 128 + share]
     remote(sp.at[:, 1 - c], sc, sc_send, sc_recv, (ep_of(0, 1), tp)).start()
 
     def term(d):
@@ -194,7 +210,7 @@
         gather_send(ch, h, k, 3, tp_of(h, back[k], 1), 1, 1, tp_of(h, 0, -1))
 
     def g_0(ch):
-        arrived(xa.at[ch, 0, :, pl.ds(0, (slots // 2 - (1 if ch == 0 else 0)) * pairs)], z_recv.at[ch])
+        arrived(xa.at[ch, 0, :, pl.ds(0, (ns - (1 if ch == 0 else 0)) * pairs)], z_recv.at[ch])
         for h in range(2):
             gather_send(ch, h, 4, 0, tp, 0, 2, tp_of(h, 1, 0))
             gather_send(ch, h, 4, 1, tp, 0, 2, tp_of(h, -1, 0))
@@ -234,7 +250,7 @@
                 gather_wait(ch, h, k, 2, 0, 1)
                 gather_wait(ch, h, k, 3, 1, 1)
 
-    xav = xa.reshape(2, n_tp, 4, half, 128)
+    xav = xa.reshape(nch, n_tp, 4, half, 128)
     width = 256
 
     def expert(ch):
@@ -280,36 +296,44 @@
             total = total + x.astype(F32)
         return total
 
-    def sum_send(ch, h, src, buf, i, base, dev_t):
-        remote(src, buf.at[ch, h, i], rs_send.at[base // 6], rs_recv.at[ch, h, base + i], (ep, dev_t)).start()
-
-    def sum_wait(ch, h, buf, i, base):
-        arrived(buf.at[ch, h, i], rs_recv.at[ch, h, base + i])
+    def landing(ch, h, i, base):
+        if base == 0:
+            return r1.at[ch, h, i], 0
+        if i in (0, 3, 4):
+            return r2t.at[ch, h, (0, 3, 4).index(i)], 1
+        return r2l.at[ch, h, (1, 2, 5).index(i)], 2
+
+    def sum_send(ch, h, src, i, base, dev_t):
+        dst, kind = landing(ch, h, i, base)
+        remote(src, dst, rs_send.at[kind], rs_recv.at[ch, h, base + i], (ep, dev_t)).start()
+
+    def sum_wait(ch, h, i, base):
+        arrived(landing(ch, h, i, base)[0], rs_recv.at[ch, h, base + i])
 
     lo, hi = pl.ds(0, 2), pl.ds(2, 2)
-    top, low = pl.ds(0, half // 2), pl.ds(half // 2, half // 2)
+    top, low = pl.ds(0, cut), pl.ds(cut, half - cut)
 
     def q_0(ch):
         for h in range(2):
-            sum_send(ch, h, pr.at[ch, h, 2, lo], r1, 0, 0, tp_of(h, 1, 0))
-            sum_send(ch, h, pr.at[ch, h, 2, hi], r1, 1, 0, tp_of(h, -1, 0))
-        for h in range(2):
-            sum_send(ch, h, pr.at[ch, h, 1, hi], r1, 2, 0, tp_of(h, 1, 0))
-            sum_send(ch, h, pr.at[ch, h, 3, lo], r1, 3, 0, tp_of(h, -1, 0))
+            sum_send(ch, h, pr.at[ch, h, 2, lo], 0, 0, tp_of(h, 1, 0))
+            sum_send(ch, h, pr.at[ch, h, 2, hi], 1, 0, tp_of(h, -1, 0))
+        for h in range(2):
+            sum_send(ch, h, pr.at[ch, h, 1, hi], 2, 0, tp_of(h, 1, 0))
+            sum_send(ch, h, pr.at[ch, h, 3, lo], 3, 0, tp_of(h, -1, 0))
 
     def q_1(ch):
         for h in range(2):
-            sum_wait(ch, h, r1, 0, 0)
+            sum_wait(ch, h, 0, 0)
             f1[ch, h, 0] = add(pr[ch, h, 1, lo], r1[ch, h, 0]).astype(BF)
-            sum_send(ch, h, f1.at[ch, h, 0], r1, 4, 0, tp_of(h, 1, 0))
-            sum_wait(ch, h, r1, 1, 0)
+            sum_send(ch, h, f1.at[ch, h, 0], 4, 0, tp_of(h, 1, 0))
+            sum_wait(ch, h, 1, 0)
             f1[ch, h, 1] = add(pr[ch, h, 3, hi], r1[ch, h, 1]).astype(BF)
-            sum_send(ch, h, f1.at[ch, h, 1], r1, 5, 0, tp_of(h, -1, 0))
+            sum_send(ch, h, f1.at[ch, h, 1], 5, 0, tp_of(h, -1, 0))
 
     def q_2(ch):
         for h in range(2):
             for i in (3, 2, 4, 5):
-                sum_wait(ch, h, r1, i, 0)
+                sum_wait(ch, h, i, 0)
             for ds in (2, 1, 3, 0):
                 pair = (4, 3) if ds < 2 else (2, 5)
                 total = add(pr[ch, h, 0, ds], r1[ch, h, pair[0], ds % 2], r1[ch, h, pair[1], ds % 2])
@@ -317,29 +341,29 @@
                     s1[ch, h, ds - 1] = total.astype(BF)
                 else:
                     s0[ch, h] = total
-            sum_send(ch, h, s1.at[ch, h, 1, top], r2, 0, 6, tp_of(h, 0, 1))
-            sum_send(ch, h, s1.at[ch, h, 1, low], r2, 1, 6, tp_of(h, 0, -1))
-            sum_send(ch, h, s1.at[ch, h, 0, low], r2, 2, 6, tp_of(h, 0, 1))
-            sum_send(ch, h, s1.at[ch, h, 2, top], r2, 3, 6, tp_of(h, 0, -1))
+            sum_send(ch, h, s1.at[ch, h, 1, top], 0, 6, tp_of(h, 0, 1))
+            sum_send(ch, h, s1.at[ch, h, 1, low], 1, 6, tp_of(h, 0, -1))
+            sum_send(ch, h, s1.at[ch, h, 0, low], 2, 6, tp_of(h, 0, 1))
+            sum_send(ch, h, s1.at[ch, h, 2, top], 3, 6, tp_of(h, 0, -1))
 
     def q_3(ch):
         for h in range(2):
-            sum_wait(ch, h, r2, 0, 6)
-            f2[ch, h, 0] = add(s1[ch, h, 0, top], r2[ch, h, 0]).astype(BF)
-            sum_send(ch, h, f2.at[ch, h, 0], r2, 4, 6, tp_of(h, 0, 1))
-            sum_wait(ch, h, r2, 1, 6)
-            f2[ch, h, 1] = add(s1[ch, h, 2, low], r2[ch, h, 1]).astype(BF)
-            sum_send(ch, h, f2.at[ch, h, 1], r2, 5, 6, tp_of(h, 0, -1))
-
-    rtv = rt.reshape(2, 2, half, 128)
+            sum_wait(ch, h, 0, 6)
+            f2t[ch, h] = add(s1[ch, h, 0, top], r2t[ch, h, 0]).astype(BF)
+            sum_send(ch, h, f2t.at[ch, h], 4, 6, tp_of(h, 0, 1))
+            sum_wait(ch, h, 1, 6)
+            f2l[ch, h] = add(s1[ch, h, 2, low], r2l[ch, h, 0]).astype(BF)
+            sum_send(ch, h, f2l.at[ch, h], 5, 6, tp_of(h, 0, -1))
+
+    rtv = rt.reshape(nch, 2, half, 128)
 
     def q_4(ch):
         for h in range(2):
             for i in (3, 2, 4, 5):
-                sum_wait(ch, h, r2, i, 6)
-            rtv[ch, h, top] = add(s0[ch, h, top], r2[ch, h, 4], r2[ch, h, 3]).astype(BF)
-            rtv[ch, h, low] = add(s0[ch, h, low], r2[ch, h, 2], r2[ch, h, 5]).astype(BF)
-        for d in order(ch)[::-1]:
+                sum_wait(ch, h, i, 6)
+            rtv[ch, h, top] = add(s0[ch, h, top], r2t[ch, h, 2], r2t[ch, h, 1]).astype(BF)
+            rtv[ch, h, low] = add(s0[ch, h, low], r2l[ch, h, 1], r2l[ch, h, 2]).astype(BF)
+        for d in groups[ch][::-1]:
             for cd in (1, 0):
                 here = pl.ds(slot_in(d, cd) * pairs, pairs)
                 there = pl.ds(((d % zs) * 2 + cd) * pairs, pairs)
@@ -358,23 +382,23 @@
 
     def product_return():
         arrived(pb.at[pl.ds(0, n_tp - 1)], pb_recv)
-        for ch in range(2):
+        for ch in range(nch):
             total = pb[0, pl.ds(ch, 1), pl.ds(0, half)]
             for t in range(1, n_tp):
                 total = total + pb[t, pl.ds(ch, 1), pl.ds(0, half)]
-            r = iota((slots // 2, half), 1)
+            r = iota((ns, half), 1)
             j = lax.shift_right_logical(r * (65536 // cap + 1), 16)
-            own = jnp.where(j == iota((slots // 2, half), 0), total, 0.0)
+            own = jnp.where(j == iota((ns, half), 0), total, 0.0)
             r = iota((half, 128), 0)
             j = lax.shift_right_logical(r * (65536 // cap + 1), 16)
             lane = jnp.where(r - cap * j == iota((half, 128), 1), 1.0, 0.0)
             table = dot(own, lane, 1, 0, HIGH)
-            for i in range(slots // 2):
-                pz[ch * (slots // 2) + i] = table[i : i + 1]
-        for ch in range(2):
-            for d in order(ch)[::-1]:
+            for i in range(ns):
+                pz[ch * ns + i] = table[i : i + 1]
+        for ch in range(nch):
+            for d in groups[ch][::-1]:
                 for cd in (1, 0):
-                    i, j = ch * (slots // 2) + slot_in(d, cd), (d % zs) * 2 + cd
+                    i, j = ch * ns + slot_in(d, cd), (d % zs) * 2 + cd
                     if d or cd:
                         remote(pz.at[i], ph.at[j], pz_send, pz_recv, (ep_of(-d, cd), tp)).start()
                     else:
@@ -385,7 +409,7 @@
             cols = pl.ds(pl.multiple_of(t * width, width), width)
             both = jnp.zeros((2 * fe, width), F32)
             last = jnp.zeros((fe, width), F32)
-            for ch in range(2):
+            for ch in range(nch):
                 x = jnp.concatenate([xav[ch, t, 0], xav[ch, t, 1]], axis=1)
                 y = jnp.concatenate([xav[ch, t, 2], xav[ch, t, 3]], axis=1)
                 both = both + dot(dlt[ch], x, 1, 0)
@@ -402,70 +426,99 @@
         dlt[ch] = dl[at, :].astype(F32).T.astype(BF)
         hdt[ch] = hd[at, :].astype(F32).T.astype(BF)
 
+    shared(0)
     g_0(0)
-    shared(0)
     g_1(0)
-    shared(1)
+    g_0(1)
     g_2(0)
-    shared(2)
-    g_0(1)
-    shared(3)
+    g_1(1)
     g_3(0)
-    g_1(1)
-    shared(4)
+    g_2(1)
+    g_0(2)
     g_4(0)
+    g_3(1)
+    g_1(2)
     g_5(0)
     for load in loads:
         load.wait()
     expert(0)
+    g_4(1)
+    g_2(2)
+    g_0(3)
+    shared(1)
+    g_5(1)
+    g_3(2)
+    parts(0)
+    g_1(3)
+    shared(2)
+    expert(1)
+    g_4(2)
+    g_2(3)
+    shared(3)
+    parts(1)
+    g_5(2)
+    g_3(3)
+    shared(4)
+    q_0(0)
+    expert(2)
+    g_4(3)
+    q_0(1)
     shared(5)
-    g_2(1)
-    parts(0)
-    g_3(1)
+    q_1(0)
+    parts(2)
+    q_0(2)
+    g_5(3)
+    q_1(1)
     shared(6)
+    expert(3)
+    parts(3)
+    q_0(3)
+    product_send()
+    q_2(0)
+    q_1(2)
+    shared(7)
+    q_2(1)
+    q_1(3)
+    shared(8)
+    q_3(0)
     turned(0)
-    g_4(1)
-    q_0(0)
-    shared(7)
-    g_5(1)
-    expert(1)
-    product_send()
-    q_1(0)
-    parts(1)
-    q_0(1)
-    shared(8)
     turned(1)
-    q_2(0)
-    weight_grads(0, 4)
-    q_1(1)
-    q_3(0)
-    weight_grads(4, 7)
+    q_2(2)
+    q_3(1)
     q_4(0)
-    q_2(1)
+    q_2(3)
+    turned(2)
+    turned(3)
+    q_3(2)
+    q_4(1)
+    weight_grads(0, 1)
+    q_3(3)
     product_return()
-    weight_grads(7, 11)
-    q_3(1)
-    weight_grads(11, 13)
-    q_4(1)
-    weight_grads(13, 16)
+    q_4(2)
+    weight_grads(1, 2)
+    q_4(3)
+    weight_grads(2, 16)
 
     e, s = tables((n_tok, rows), 1)
-    r0, r1c = routes[:, 0:1], routes[:, 1:2]
+    def turn(row):
+        return jnp.broadcast_to(row, (n_tok, n_tok)).T
+
+    r0, r1c = (turn(routes_t[k : k + 1, :].astype(F32))[:, 0:1].astype(jnp.int32) for k in range(2))
     hit = (r0 == e) | (r1c == e)
     cm[...] = flag(hit & (dot(after, flag(hit), 1, 0) == s))
     j = iota((n_tok, slots), 1)
     ej = lax.bitwise_and(z + lax.shift_right_logical(j, 1), zs - 1) * 2 + lax.bitwise_and(c + j, 1)
     seen = dot(after, flag((r0 == ej) | (r1c == ej)), 1, 0)
-    wc = weight(rw[...])
     arrived(ph.at[pl.ds(0, slots - 1)], pz_recv)
     table = jnp.concatenate([ph[i] for i in range(slots)], axis=0)
     for k in range(2):
-        mine = routes[:, k : k + 1] == ej
+        mine = (r0, r1c)[k] == ej
         rank = jnp.sum(jnp.where(mine, seen, 0.0), axis=1, keepdims=True)
         found = dot(jnp.where(mine, 1.0, 0.0), table, 1, 0, HIGH)
         lane = iota((n_tok, 128), 1).astype(F32)
         value = jnp.sum(jnp.where(lane == rank, found, 0.0), axis=1, keepdims=True)
-        wg_o[:, k : k + 1] = value / wc[:, k : k + 1]
+        row = jnp.broadcast_to(value, (n_tok, n_tok)).T[0:1]
+        wg_o[k : k + 1, :] = row / wt[k : k + 1, :]
     arrived(rh.at[:, pl.ds(0, (slots - 1) * pairs)], rz_recv)
     rhv = rh.reshape(2, rows, 128)
     for h in range(2):
@@ -474,7 +527,8 @@
     left(sb.at[:, pl.ds(0, (slots - 1) * pairs)], z_send)
     left(xa.at[:, pl.ds(0, n_tp - 1)], ag_send)
     left(r1, rs_send.at[0])
-    left(r2, rs_send.at[1])
+    left(r2t, rs_send.at[1])
+    left(r2l, rs_send.at[2])
     left(rh.at[:, pl.ds(0, (slots - 1) * pairs)], rz_send)
     left(pb.at[pl.ds(0, n_tp - 1)], pb_send)
     left(ph.at[pl.ds(0, slots - 1)], pz_send)
@@ -484,51 +538,74 @@
             left(shs.at[way, step], sh_send.at[way, step])
 
 
+def settle(*refs):
+    n = len(refs) // 3
+    src, dst, held, sems = refs[:n], refs[n : 2 * n], refs[2 * n : 3 * n], refs[3 * n :]
+    into = [pltpu.make_async_copy(src[i], held[i], sems[0].at[i]) for i in range(n)]
+    out = [pltpu.make_async_copy(held[i], dst[i], sems[1].at[i]) for i in range(n)]
+    for copy in into:
+        copy.start()
+    for i in range(n):
+        into[i].wait()
+        out[i].start()
+    for copy in out:
+        copy.wait()
+
+
 def local(zs, tokens, out_grad, routes, route_weights, gate_proj, up_proj, down_proj, shared_hidden):
     n_tok, feat = tokens.shape
     _, fe, width = gate_proj.shape
     slots = 2 * zs
     cap = max(2, 5 * n_tok * routes.shape[1] // (4 * slots))
     rows = slots * cap
-    half = rows // 2
+    nch = len(chunks_of(zs))
+    half = rows // nch
+    cut = (half // 2 + 15) // 16 * 16
     n_tp = SIDE * SIDE
     share = shared_hidden.shape[1] // slots
     far = zs // 2
     vmem = pl.BlockSpec(memory_space=pltpu.VMEM)
-    hbm = pl.BlockSpec(memory_space=pl.ANY)
+    hbm = pl.BlockSpec(memory_space=pltpu.HBM)
     dma = pltpu.SemaphoreType.DMA
     V = pltpu.VMEM
     out = pl.pallas_call(
         functools.partial(kernel, zs, cap),
         out_shape=(
             jax.ShapeDtypeStruct((n_tok, feat), BF),
-            jax.ShapeDtypeStruct((n_tok, 2), F32),
+            jax.ShapeDtypeStruct((2, n_tok), F32),
             jax.ShapeDtypeStruct((fe, width), BF),
             jax.ShapeDtypeStruct((fe, width), BF),
             jax.ShapeDtypeStruct((fe, width), BF),
             jax.ShapeDtypeStruct((share, feat), F32),
         ),
-        in_specs=[vmem] * 6 + [hbm] * 3 + [vmem],
+        in_specs=[hbm] * 8,
         out_specs=(vmem,) * 6,
         scratch_shapes=[
+            V((n_tok, feat), BF),
+            V((n_tok, feat), BF),
+            V((2, n_tok), jnp.int32),
+            V((2, n_tok), F32),
+            V(shared_hidden.shape, BF),
             V((2 * fe, width), BF),
             V((fe, width), BF),
             V((4, rows // 2, 2, 128), BF),
-            V((2, n_tp, 4, half // 2, 2, 128), BF),
+            V((nch, n_tp, 4, half // 2, 2, 128), BF),
             V((rows, 2 * fe), BF),
             V((rows, fe), BF),
-            V((2, 2 * fe, half), BF),
-            V((2, fe, half), BF),
-            V((2, 2, SIDE, SIDE, half, 128), BF),
-            V((2, 2, 6, 2, half, 128), BF),
-            V((2, 2, 2, 2, half, 128), BF),
-            V((2, 2, half, 128), F32),
-            V((2, 2, 3, half, 128), BF),
-            V((2, 2, 6, half // 2, 128), BF),
-            V((2, 2, 2, half // 2, 128), BF),
-            V((2, 2, half // 2, 2, 128), BF),
+            V((nch, 2 * fe, half), BF),
+            V((nch, fe, half), BF),
+            V((nch, 2, SIDE, SIDE, half, 128), BF),
+            V((nch, 2, 6, 2, half, 128), BF),
+            V((nch, 2, 2, 2, half, 128), BF),
+            V((nch, 2, half, 128), F32),
+            V((nch, 2, 3, half, 128), BF),
+            V((nch, 2, 3, cut, 128), BF),
+            V((nch, 2, 3, half - cut, 128), BF),
+            V((nch, 2, cut, 128), BF),
+            V((nch, 2, half - cut, 128), BF),
+            V((nch, 2, half // 2, 2, 128), BF),
             V((2, rows // 2, 2, 128), BF),
-            V((n_tp, 2, 256), F32),
+            V((n_tp, nch, (half + 127) // 128 * 128), F32),
             V((slots, 1, 128), F32),
             V((slots, 1, 128), F32),
             V((n_tok, rows), BF),
@@ -536,23 +613,30 @@
             V((zs, share, feat), F32),
             V((2, far, share, feat), F32),
             V((2, far, share, feat), F32),
-            dma((3,)),
-            dma, dma((2,)),
-            dma, dma((2, 2, 5, 4)),
-            dma((2,)), dma((2, 2, 12)),
+            dma((8,)),
+            dma, dma((nch,)),
+            dma, dma((nch, 2, 5, 4)),
+            dma((3,)), dma((nch, 2, 12)),
             dma, dma,
             dma, dma,
             dma, dma,
             dma, dma,
             dma((2, far)), dma((2, far)),
         ],
-        compiler_params=pltpu.CompilerParams(collective_id=0, has_side_effects=True),
+        compiler_params=pltpu.CompilerParams(collective_id=0, has_side_effects=True, vmem_limit_bytes=60 * 1024 * 1024),
     )(
-        tokens, out_grad, routes, routes.T, route_weights, route_weights.T,
+        tokens, out_grad, routes.T, route_weights.T,
         gate_proj[0], up_proj[0], down_proj[0], shared_hidden,
     )
-    tg, wg, gg, ug, dg, sg = out
-    return tg, wg, gg[None], ug[None], dg[None], sg
+    shapes = [jax.ShapeDtypeStruct(a.shape, a.dtype) for a in out]
+    tg, wg, gg, ug, dg, sg = pl.pallas_call(
+        settle,
+        out_shape=shapes,
+        in_specs=[hbm] * len(out),
+        out_specs=[hbm] * len(out),
+        scratch_shapes=[V(a.shape, a.dtype) for a in out] + [dma((len(out),)), dma((len(out),))],
+    )(*out)
+    return tg, wg.T, gg[None], ug[None], dg[None], sg
 
 
 def solution(mesh):

time: 105 us -> 93.4 us (0.89)
  local copies, waits for them, and re-layouts: 8.87 us -> 0 us
  Pallas kernels: 95.3 us -> 92.6 us
    unnamed x20 -> x0, local copies, waits for them, and re-layouts: 8.87 us -> none
    pallas_call x1, Pallas kernels: 95.3 us -> 90.2 us  [local(): pl.pallas_call(functools.partial(kernel, zs, cap), out_shape=(jax.ShapeDt...]
    pallas_call x0 -> x1, Pallas kernels: none -> 2.33 us  [local(): pl.pallas_call(settle, out_shape=shapes, in_specs=[hbm] * len(out), out_s...]
where the time goes in v2:
time: 93.4 us; the launch traced here: 93.2 us
  Pallas kernels  92.6 us (99%)
    pallas_call x1, Pallas kernels, local(): pl.pallas_call(functools.partial(kernel, zs, cap), out_shape=(jax.ShapeDt...  90.2 us
    pallas_call x1, Pallas kernels, local(): pl.pallas_call(settle, out_shape=shapes, in_specs=[hbm] * len(out), out_s...  2.33 us

profile of v2, /device:TPU:1, one launch (start us, length us, event | category | flops | bytes accessed | tf_op | source)
XLA Modules:
  0.0 93.2 jit_solution(5776947573704722435)
XLA Ops:
  0.6 90.2 %shard_map.127 = (bf16[128,256]{1,0:T(8,128)(2,1)}, f32[2,128]{1,0:T(2,128)}, bf16[64,4096]{1,0:T(8,128)(2,1)}, bf16[64,4096]{1,0:T(8,128)(2,1)}, bf16[64,4096]{1,0:T(8,128)(2,1)}, /*index=5*/f32[32,256]{1,0:T(8,128)}) custom-call(bf16[128,256]{1,0:T(8,128)(2,1)} %tok_h.1, bf16[128,256]{1,0:T(8,128)(2,1)} %og_h.1, s32[2,128]{1,0:T(2,128)} %bitcast.12, ...), custom_call_target="tpu_custom_call" | custom-call | tf_op jit(solution)/shard_map/pallas_call | solution.py:571
  90.9 2.3 %shard_map.128 = (bf16[128,256]{1,0:T(8,128)(2,1)}, f32[2,128]{1,0:T(2,128)}, bf16[64,4096]{1,0:T(8,128)(2,1)}, bf16[64,4096]{1,0:T(8,128)(2,1)}, bf16[64,4096]{1,0:T(8,128)(2,1)}, /*index=5*/f32[32,256]{1,0:T(8,128)}) custom-call(bf16[128,256]{1,0:T(8,128)(2,1)} %get-tuple-element.18.refs_0_, f32[2,128]{1,0:T(2,128)} %get-tuple-element.19.refs_1_, ...), custom_call_target="tpu_custom_call" | custom-call | tf_op jit(solution)/shard_map/pallas_call | solution.py:632

commit v3 on v2

--- a/solution.py
+++ b/solution.py
@@ -11,7 +11,7 @@
 BF = jnp.bfloat16
 F32 = jnp.float32
 SIDE = 4
-ORDER = (0, 1, 2, 3)
+ORDER = (0, 3, 2, 1)
 HIGH = lax.Precision.HIGHEST
 
 
@@ -36,8 +36,8 @@
     zs, cap,
     tok_h, og_h, routes_h, rw_h, gate, up, down, sh_h,
     tg_o, wg_o, gg_o, ug_o, dg_o, sg_o,
-    tok, og, routes_t, rw_t, sh, wgu, wdn, sb, xa, dl, hd, dlt, hdt, pr, r1, f1, s0, s1, r2t, r2l, f2t, f2l, rt, rh, pb, pz, ph, cm,
-    sp, sc, shb, shs,
+    tok, og, routes_t, rw_t, sh, wgu, wdn, sb, xa, dl, hd, dlt, hdt, pr, r1, f1, s0, s1, r2, rt, rh, pb, pz, ph, cm,
+    sp, sc, shb, shs, ea, eb,
     w_sem, z_send, z_recv, ag_send, ag_recv, rs_send, rs_recv, rz_send, rz_recv,
     pb_send, pb_recv, pz_send, pz_recv, sc_send, sc_recv, sh_send, sh_recv,
 ):
@@ -51,7 +51,6 @@
     nch = len(groups)
     ns = slots // nch
     half = rows // nch
-    cut = (half // 2 + 15) // 16 * 16
     pairs = cap // 2
     fe = gate.shape[0]
     n_tok = tok.shape[0]
@@ -244,16 +243,31 @@
         for h in range(2):
             relay(ch, h, 3)
 
-    def g_5(ch):
-        for h in range(2):
-            for k in range(4):
+    def g_5(ch, ks=range(4)):
+        for h in range(2):
+            for k in ks:
                 gather_wait(ch, h, k, 2, 0, 1)
                 gather_wait(ch, h, k, 3, 1, 1)
 
     xav = xa.reshape(nch, n_tp, 4, half, 128)
     width = 256
 
-    def expert(ch):
+    def early(ch, dps, start):
+        a, b = start
+        for dp in dps:
+            for ds in range(SIDE):
+                t, u = tp_of(0, dp, ds), tp_of(1, dp, ds)
+                x = jnp.concatenate([xav[ch, t, 0], xav[ch, t, 1]], axis=1)
+                y = jnp.concatenate([xav[ch, u, 2], xav[ch, u, 3]], axis=1)
+                a = a + dot(x, wgu[:, pl.ds(pl.multiple_of(t * width, width), width)], 1, 1)
+                b = b + dot(y, wdn[:, pl.ds(pl.multiple_of(u * width, width), width)], 1, 1)
+        return a, b
+
+    def expert_early(ch):
+        start = (jnp.zeros((half, 2 * fe), F32), jnp.zeros((half, fe), F32))
+        ea[...], eb[...] = early(ch, (0, -1, 1), start)
+
+    def expert(ch, late=False):
         def sums(i, total):
             a, b = total
             for u in range(4):
@@ -266,7 +280,10 @@
             return a, b
 
         start = (jnp.zeros((half, 2 * fe), F32), jnp.zeros((half, fe), F32))
-        gu, back_grad = lax.fori_loop(0, n_tp // 4, sums, start)
+        if late:
+            gu, back_grad = early(ch, (2,), (ea[...], eb[...]))
+        else:
+            gu, back_grad = lax.fori_loop(0, n_tp // 4, sums, start)
         pre_gate, pre_up = gu[:, :fe], gu[:, fe:]
         squash = 1.0 / (1.0 + jnp.exp(-pre_gate))
         activated = pre_gate * squash
@@ -280,10 +297,12 @@
         line = dot(jnp.ones((8, fe), F32), product, 1, 1, HIGH)
         pb[tp, pl.ds(ch, 1), pl.ds(0, half)] = line[0:1]
 
-    def parts(ch):
+    def parts(ch, which=(True, False)):
         at = pl.ds(ch * half, half)
         for dy in range(SIDE):
             for dx in range(SIDE):
+                if (2 in (dx, dy)) not in which:
+                    continue
                 t = tp_of(0, dx, dy)
                 cols = pl.ds(pl.multiple_of(t * width, width), width)
                 out = dot(dl[at, :], wgu[:, cols], 1, 0).astype(BF)
@@ -297,26 +316,26 @@
         return total
 
     def landing(ch, h, i, base):
-        if base == 0:
-            return r1.at[ch, h, i], 0
-        if i in (0, 3, 4):
-            return r2t.at[ch, h, (0, 3, 4).index(i)], 1
-        return r2l.at[ch, h, (1, 2, 5).index(i)], 2
+        return (r1 if base == 0 else r2).at[ch, h, i]
 
     def sum_send(ch, h, src, i, base, dev_t):
-        dst, kind = landing(ch, h, i, base)
-        remote(src, dst, rs_send.at[kind], rs_recv.at[ch, h, base + i], (ep, dev_t)).start()
+        remote(src, landing(ch, h, i, base), rs_send.at[base // 6], rs_recv.at[ch, h, base + i], (ep, dev_t)).start()
 
     def sum_wait(ch, h, i, base):
-        arrived(landing(ch, h, i, base)[0], rs_recv.at[ch, h, base + i])
+        arrived(landing(ch, h, i, base), rs_recv.at[ch, h, base + i])
 
     lo, hi = pl.ds(0, 2), pl.ds(2, 2)
-    top, low = pl.ds(0, cut), pl.ds(cut, half - cut)
 
     def q_0(ch):
+        q_0a(ch)
+        q_0b(ch)
+
+    def q_0a(ch):
         for h in range(2):
             sum_send(ch, h, pr.at[ch, h, 2, lo], 0, 0, tp_of(h, 1, 0))
             sum_send(ch, h, pr.at[ch, h, 2, hi], 1, 0, tp_of(h, -1, 0))
+
+    def q_0b(ch):
         for h in range(2):
             sum_send(ch, h, pr.at[ch, h, 1, hi], 2, 0, tp_of(h, 1, 0))
             sum_send(ch, h, pr.at[ch, h, 3, lo], 3, 0, tp_of(h, -1, 0))
@@ -341,28 +360,16 @@
                     s1[ch, h, ds - 1] = total.astype(BF)
                 else:
                     s0[ch, h] = total
-            sum_send(ch, h, s1.at[ch, h, 1, top], 0, 6, tp_of(h, 0, 1))
-            sum_send(ch, h, s1.at[ch, h, 1, low], 1, 6, tp_of(h, 0, -1))
-            sum_send(ch, h, s1.at[ch, h, 0, low], 2, 6, tp_of(h, 0, 1))
-            sum_send(ch, h, s1.at[ch, h, 2, top], 3, 6, tp_of(h, 0, -1))
-
-    def q_3(ch):
-        for h in range(2):
-            sum_wait(ch, h, 0, 6)
-            f2t[ch, h] = add(s1[ch, h, 0, top], r2t[ch, h, 0]).astype(BF)
-            sum_send(ch, h, f2t.at[ch, h], 4, 6, tp_of(h, 0, 1))
-            sum_wait(ch, h, 1, 6)
-            f2l[ch, h] = add(s1[ch, h, 2, low], r2l[ch, h, 0]).astype(BF)
-            sum_send(ch, h, f2l.at[ch, h], 5, 6, tp_of(h, 0, -1))
+            for i, ds in ((1, 2), (0, 1), (2, -1)):
+                sum_send(ch, h, s1.at[ch, h, i], i, 6, tp_of(h, 0, ds))
 
     rtv = rt.reshape(nch, 2, half, 128)
 
     def q_4(ch):
         for h in range(2):
-            for i in (3, 2, 4, 5):
+            for i in (0, 2, 1):
                 sum_wait(ch, h, i, 6)
-            rtv[ch, h, top] = add(s0[ch, h, top], r2t[ch, h, 2], r2t[ch, h, 1]).astype(BF)
-            rtv[ch, h, low] = add(s0[ch, h, low], r2l[ch, h, 1], r2l[ch, h, 2]).astype(BF)
+            rtv[ch, h] = add(s0[ch, h], r2[ch, h, 0], r2[ch, h, 2], r2[ch, h, 1]).astype(BF)
         for d in groups[ch][::-1]:
             for cd in (1, 0):
                 here = pl.ds(slot_in(d, cd) * pairs, pairs)
@@ -429,70 +436,70 @@
     shared(0)
     g_0(0)
     g_1(0)
+    g_2(0)
     g_0(1)
-    g_2(0)
+    g_3(0)
     g_1(1)
-    g_3(0)
-    g_2(1)
     g_0(2)
     g_4(0)
-    g_3(1)
+    g_0(3)
+    shared(1)
+    g_2(1)
     g_1(2)
     g_5(0)
     for load in loads:
         load.wait()
     expert(0)
+    shared(2)
+    g_1(3)
+    g_3(1)
+    g_2(2)
+    shared(3)
+    parts(0)
     g_4(1)
-    g_2(2)
-    g_0(3)
-    shared(1)
+    g_2(3)
+    g_3(2)
+    shared(4)
     g_5(1)
-    g_3(2)
-    parts(0)
-    g_1(3)
-    shared(2)
+    g_3(3)
+    g_4(2)
     expert(1)
-    g_4(2)
-    g_2(3)
-    shared(3)
+    shared(5)
+    g_4(3)
+    q_0(0)
     parts(1)
+    q_0(1)
     g_5(2)
-    g_3(3)
-    shared(4)
-    q_0(0)
+    shared(6)
     expert(2)
-    g_4(3)
-    q_0(1)
-    shared(5)
     q_1(0)
     parts(2)
     q_0(2)
-    g_5(3)
     q_1(1)
-    shared(6)
-    expert(3)
-    parts(3)
-    q_0(3)
+    g_5(3, (0, 1, 2))
+    shared(7)
+    expert_early(3)
+    g_5(3, (3,))
+    expert(3, True)
+    parts(3, (True,))
+    q_0a(3)
+    parts(3, (False,))
+    q_0b(3)
     product_send()
     q_2(0)
     q_1(2)
-    shared(7)
     q_2(1)
     q_1(3)
     shared(8)
-    q_3(0)
+    q_4(0)
     turned(0)
     turned(1)
     q_2(2)
-    q_3(1)
-    q_4(0)
+    q_4(1)
     q_2(3)
     turned(2)
     turned(3)
-    q_3(2)
-    q_4(1)
     weight_grads(0, 1)
-    q_3(3)
     product_return()
     q_4(2)
     weight_grads(1, 2)
@@ -527,8 +534,7 @@
     left(sb.at[:, pl.ds(0, (slots - 1) * pairs)], z_send)
     left(xa.at[:, pl.ds(0, n_tp - 1)], ag_send)
     left(r1, rs_send.at[0])
-    left(r2t, rs_send.at[1])
-    left(r2l, rs_send.at[2])
+    left(r2, rs_send.at[1])
     left(rh.at[:, pl.ds(0, (slots - 1) * pairs)], rz_send)
     left(pb.at[pl.ds(0, n_tp - 1)], pb_send)
     left(ph.at[pl.ds(0, slots - 1)], pz_send)
@@ -560,7 +566,6 @@
     rows = slots * cap
     nch = len(chunks_of(zs))
     half = rows // nch
-    cut = (half // 2 + 15) // 16 * 16
     n_tp = SIDE * SIDE
     share = shared_hidden.shape[1] // slots
     far = zs // 2
@@ -599,10 +604,7 @@
             V((nch, 2, 2, 2, half, 128), BF),
             V((nch, 2, half, 128), F32),
             V((nch, 2, 3, half, 128), BF),
-            V((nch, 2, 3, cut, 128), BF),
-            V((nch, 2, 3, half - cut, 128), BF),
-            V((nch, 2, cut, 128), BF),
-            V((nch, 2, half - cut, 128), BF),
+            V((nch, 2, 3, half, 128), BF),
             V((nch, 2, half // 2, 2, 128), BF),
             V((2, rows // 2, 2, 128), BF),
             V((n_tp, nch, (half + 127) // 128 * 128), F32),
@@ -613,10 +615,12 @@
             V((zs, share, feat), F32),
             V((2, far, share, feat), F32),
             V((2, far, share, feat), F32),
+            V((half, 2 * fe), F32),
+            V((half, fe), F32),
             dma((8,)),
             dma, dma((nch,)),
             dma, dma((nch, 2, 5, 4)),
-            dma((3,)), dma((nch, 2, 12)),
+            dma((2,)), dma((nch, 2, 9)),
             dma, dma,
             dma, dma,
             dma, dma,

time: 93.4 us -> 87 us (0.931)
  Pallas kernels: 92.6 us -> 86.2 us
    pallas_call x1, Pallas kernels: 90.2 us -> 83.9 us  [local(): pl.pallas_call(functools.partial(kernel, zs, cap), out_shape=(jax.ShapeDt...]
where the time goes in v3:
time: 87 us; the launch traced here: 86.8 us
  Pallas kernels  86.2 us (99%)
    pallas_call x1, Pallas kernels, local(): pl.pallas_call(functools.partial(kernel, zs, cap), out_shape=(jax.ShapeDt...  83.9 us
    pallas_call x1, Pallas kernels, local(): pl.pallas_call(settle, out_shape=shapes, in_specs=[hbm] * len(out), out_s...  2.33 us

profile of v3, /device:TPU:1, one launch (start us, length us, event | category | flops | bytes accessed | tf_op | source)
XLA Modules:
  0.0 86.8 jit_solution(10607025040411433116)
XLA Ops:
  0.6 83.9 %shard_map.127 = (bf16[128,256]{1,0:T(8,128)(2,1)}, f32[2,128]{1,0:T(2,128)}, bf16[64,4096]{1,0:T(8,128)(2,1)}, bf16[64,4096]{1,0:T(8,128)(2,1)}, bf16[64,4096]{1,0:T(8,128)(2,1)}, /*index=5*/f32[32,256]{1,0:T(8,128)}) custom-call(bf16[128,256]{1,0:T(8,128)(2,1)} %tok_h.1, bf16[128,256]{1,0:T(8,128)(2,1)} %og_h.1, s32[2,128]{1,0:T(2,128)} %bitcast.12, ...), custom_call_target="tpu_custom_call" | custom-call | tf_op jit(solution)/shard_map/pallas_call | solution.py:576
  84.5 2.3 %shard_map.128 = (bf16[128,256]{1,0:T(8,128)(2,1)}, f32[2,128]{1,0:T(2,128)}, bf16[64,4096]{1,0:T(8,128)(2,1)}, bf16[64,4096]{1,0:T(8,128)(2,1)}, bf16[64,4096]{1,0:T(8,128)(2,1)}, /*index=5*/f32[32,256]{1,0:T(8,128)}) custom-call(bf16[128,256]{1,0:T(8,128)(2,1)} %get-tuple-element.18.refs_0_, f32[2,128]{1,0:T(2,128)} %get-tuple-element.19.refs_1_, ...), custom_call_target="tpu_custom_call" | custom-call | tf_op jit(solution)/shard_map/pallas_call | solution.py:636

commit v4 on v3

--- a/solution.py
+++ b/solution.py
@@ -35,8 +35,8 @@
 def kernel(
     zs, cap,
     tok_h, og_h, routes_h, rw_h, gate, up, down, sh_h,
-    tg_o, wg_o, gg_o, ug_o, dg_o, sg_o,
-    tok, og, routes_t, rw_t, sh, wgu, wdn, sb, xa, dl, hd, dlt, hdt, pr, r1, f1, s0, s1, r2, rt, rh, pb, pz, ph, cm,
+    tg_o, wg_o, gg_h, ug_h, dg_h, sg_o,
+    gg_o, ug_o, dg_o, g_sem, tok, og, routes_t, rw_t, sh, wgu, wdn, sb, xa, dl, hd, dlt, hdt, pr, r1, f1, s0, s1, r2, rt, rh, pb, pz, ph, cm,
     sp, sc, shb, shs, ea, eb,
     w_sem, z_send, z_recv, ag_send, ag_recv, rs_send, rs_recv, rz_send, rz_recv,
     pb_send, pb_recv, pz_send, pz_recv, sc_send, sc_recv, sh_send, sh_recv,
@@ -516,6 +516,12 @@
     j = iota((n_tok, slots), 1)
     ej = lax.bitwise_and(z + lax.shift_right_logical(j, 1), zs - 1) * 2 + lax.bitwise_and(c + j, 1)
     seen = dot(after, flag((r0 == ej) | (r1c == ej)), 1, 0)
+    stores = [
+        pltpu.make_async_copy(src, dst, g_sem.at[i])
+        for i, (src, dst) in enumerate(((gg_o, gg_h), (ug_o, ug_h), (dg_o, dg_h)))
+    ]
+    for store in stores:
+        store.start()
     arrived(ph.at[pl.ds(0, slots - 1)], pz_recv)
     table = jnp.concatenate([ph[i] for i in range(slots)], axis=0)
     for k in range(2):
@@ -531,6 +537,8 @@
     for h in range(2):
         tg_o[:, h * 128 : (h + 1) * 128] = dot(cm[...], rhv[h], 1, 0).astype(BF)
 
+    for store in stores:
+        store.wait()
     left(sb.at[:, pl.ds(0, (slots - 1) * pairs)], z_send)
     left(xa.at[:, pl.ds(0, n_tp - 1)], ag_send)
     left(r1, rs_send.at[0])
@@ -584,8 +592,12 @@
             jax.ShapeDtypeStruct((share, feat), F32),
         ),
         in_specs=[hbm] * 8,
-        out_specs=(vmem,) * 6,
+        out_specs=(vmem, vmem, hbm, hbm, hbm, vmem),
         scratch_shapes=[
+            V((fe, width), BF),
+            V((fe, width), BF),
+            V((fe, width), BF),
+            dma((3,)),
             V((n_tok, feat), BF),
             V((n_tok, feat), BF),
             V((2, n_tok), jnp.int32),

time: 87 us -> 86.5 us (level)
  no operation moved by 1% of the time
where the time goes in v4:
time: 86.5 us; the launch traced here: 86.3 us
  Pallas kernels  85.7 us (99%)
    pallas_call x1, Pallas kernels, local(): pl.pallas_call(functools.partial(kernel, zs, cap), out_shape=(jax.ShapeDt...  83.4 us
    pallas_call x1, Pallas kernels, local(): pl.pallas_call(settle, out_shape=shapes, in_specs=[hbm] * len(out), out_s...  2.33 us

profile of v4, /device:TPU:1, one launch (start us, length us, event | category | flops | bytes accessed | tf_op | source)
XLA Modules:
  0.0 86.3 jit_solution(3970302297603700426)
XLA Ops:
  0.6 83.4 %shard_map.127 = (bf16[128,256]{1,0:T(8,128)(2,1)}, f32[2,128]{1,0:T(2,128)}, bf16[64,4096]{1,0:T(8,128)(2,1)}, bf16[64,4096]{1,0:T(8,128)(2,1)}, bf16[64,4096]{1,0:T(8,128)(2,1)}, /*index=5*/f32[32,256]{1,0:T(8,128)}) custom-call(bf16[128,256]{1,0:T(8,128)(2,1)} %tok_h.1, bf16[128,256]{1,0:T(8,128)(2,1)} %og_h.1, s32[2,128]{1,0:T(2,128)} %bitcast.12, ...), custom_call_target="tpu_custom_call" | custom-call | tf_op jit(solution)/shard_map/pallas_call | solution.py:584
  84.0 2.3 %shard_map.128 = (bf16[128,256]{1,0:T(8,128)(2,1)}, f32[2,128]{1,0:T(2,128)}, bf16[64,4096]{1,0:T(8,128)(2,1)}, bf16[64,4096]{1,0:T(8,128)(2,1)}, bf16[64,4096]{1,0:T(8,128)(2,1)}, /*index=5*/f32[32,256]{1,0:T(8,128)}) custom-call(bf16[128,256]{1,0:T(8,128)(2,1)} %get-tuple-element.18.refs_0_, f32[2,128]{1,0:T(2,128)} %get-tuple-element.19.refs_1_, ...), custom_call_target="tpu_custom_call" | custom-call | tf_op jit(solution)/shard_map/pallas_call | solution.py:648
